TPU v7x, 256 devices: a whole 4x4x8 slice. The times are simulated.
256 devices in a mesh: sp: 64 (over z, x, core), tp: 4 (over y).
Axes of the slice: x: 4, y: 4, z: 8, core: 2. Of those that a mesh axis runs over, the one named last changes fastest.
Arguments:
- query_wide: bfloat16 [8192, 1536], P('sp', 'tp'), may hold values from -600 to 600
- query_narrow: bfloat16 [8192, 1024], P('sp', 'tp'), may hold values from -600 to 600
- latent: bfloat16 [8192, 512], P('sp'), may hold values from -6 to 6
- rope_key: bfloat16 [8192, 64], P('sp'), may hold values from -6 to 6
- latent_norm_weight: float32 [512], replicated, may hold values from 0.1 to 1.9
- broad_key_lift: bfloat16 [512, 1024], P(None, 'tp'), may hold values from -0.25 to 0.25
- broad_value_lift: bfloat16 [512, 1024], P(None, 'tp'), may hold values from -0.25 to 0.25
- slim_key_lift: bfloat16 [512, 512], P(None, 'tp'), may hold values from -0.25 to 0.25
- slim_value_lift: bfloat16 [512, 512], P(None, 'tp'), may hold values from -0.25 to 0.25
- out_wide: bfloat16 [1024, 2048], P('tp'), may hold values from -0.4375 to 0.4375
- out_narrow: bfloat16 [512, 2048], P('tp'), may hold values from -0.4375 to 0.4375
- resid: bfloat16 [8192, 2048], P('sp'), may hold values from -20 to 20
- ffn_gain: float32 [2048], replicated, may hold values from 0.1 to 1.9
- group_route: int32 [8192], P('sp'), may hold values from 0 to 63, as said below
- expert_pair: int32 [8192, 2], P('sp'), may hold values from 0 to 3, all different within a row
- group_prob: float32 [8192], P('sp'), may hold values from 0.2 to 1
- expert_prob: float32 [8192, 2], P('sp'), may hold values from 0.05 to 1
- gate_weight: bfloat16 [64, 4, 2048, 512], P('sp', None, None, 'tp'), may hold values from -0.125 to 0.125
- up_weight: bfloat16 [64, 4, 2048, 512], P('sp', None, None, 'tp'), may hold values from -0.125 to 0.125
- down_weight: bfloat16 [64, 4, 512, 2048], P('sp', None, 'tp'), may hold values from -0.25 to 0.25
Outputs:
- mixed: bfloat16 [8192, 2048], P('sp', 'tp')
Inputs may be any that keep to these rules, and one draw needn't show every extreme that they name: `group_route`: of the 128 tokens of one index of sp at most 4 name one group; in every draw one group is named by exactly 4 tokens of every index of sp, and every index of sp names one more group exactly 4 times. `expert_pair`: A token's two experts are different.
All inputs are finite; a program needn't handle non-finite values.
Results may differ from a plain program's by a relative error of at most 0.017.
Values may be sent and summed in bfloat16 or wider, within the bound.
A program may use at most 128 MiB of HBM per device.

v0:
```python
import math

import jax
import jax.numpy as jnp
from jax import lax
from jax.sharding import PartitionSpec as P

PLAIN_WIDTH_WIDE = 128
PLAIN_WIDTH_SLIM = 64
ROPE = 64
VALUE_WIDTH_WIDE = 128
VALUE_WIDTH_SLIM = 64
EPG = 4


ROPE_BASE = 10000.0
EPSILON = 1e-06
MASKED = -1e30


def sent_together(arrays, axis, dim, along):
    widths = [a.shape[along] for a in arrays]
    both = jnp.concatenate(arrays, axis=along)
    result = lax.all_gather(both, axis, axis=dim, tiled=True)
    return tuple(jnp.split(result, [sum(widths[:k]) for k in range(1, len(widths))], axis=along))


def in_blocks(x, dim, peers):
    before, after = (x.shape[:dim], x.shape[dim + 1 :])
    return jnp.moveaxis(x.reshape(*before, peers, -1, *after), dim, 0)


def sum_at_owner(x, axis, dim):
    blocks = in_blocks(x, dim, lax.axis_size(axis))
    arrived = lax.all_to_all(blocks, axis, split_axis=0, concat_axis=0, tiled=True)
    return arrived.astype(jnp.float32).sum(axis=0)


def sent_to_all(x, axis):
    copies = jnp.broadcast_to(x, (lax.axis_size(axis), *x.shape))
    return lax.all_to_all(copies, axis, split_axis=0, concat_axis=0, tiled=True)


def of_everyone(x, axis):
    everything = sent_to_all(x, axis)
    return jnp.sum(everything, axis=0)


def joined_along(blocks, dim):
    blocks = jnp.moveaxis(blocks, 0, dim)
    shape = blocks.shape
    return blocks.reshape(*shape[:dim], shape[dim] * shape[dim + 1], *shape[dim + 2 :])


def gathered_copies(x, axis, dim):
    blocks = sent_to_all(x, axis)
    return joined_along(blocks, dim)


def rms_scale(values, gain_row):
    widened = values.astype(jnp.float32)
    return (
        widened
        * lax.rsqrt(jnp.mean(widened * widened, axis=-1, keepdims=True) + EPSILON)
        * gain_row
    )


def angles(positions, width):
    frequency = 1.0 / ROPE_BASE ** (jnp.arange(0, width, 2).astype(jnp.float32) / width)
    return positions.astype(jnp.float32)[:, None] * frequency[None, :]


def rotary(values, angle_table):
    half_width = values.shape[-1] // 2
    first_half = values[..., :half_width]
    second = values[..., half_width:]
    return jnp.concatenate(
        [
            first_half * jnp.cos(angle_table) - second * jnp.sin(angle_table),
            second * jnp.cos(angle_table) + first_half * jnp.sin(angle_table),
        ],
        axis=-1,
    )


def split_query(queries, head_count, nope_width, angle_table):
    shaped = queries.reshape(queries.shape[0], head_count, nope_width + ROPE)
    turned = rotary(shaped[..., nope_width:].astype(jnp.float32), angle_table[:, None, :]).astype(
        jnp.bfloat16
    )
    return (shaped[..., :nope_width], turned)


def group_step(
    carry_state, query_pair, key_block, value_block, rot_block, key_pos, query_pos, scale
):
    row_peak, row_total, accum_out = carry_state
    scores = jnp.einsum(
        "thd,khd->htk", query_pair[0], key_block, preferred_element_type=jnp.float32
    )
    scores = scores + jnp.einsum(
        "thd,kd->htk", query_pair[1], rot_block, preferred_element_type=jnp.float32
    )
    scores = jnp.where((query_pos[:, None] >= key_pos[None, :])[None], scores * scale, MASKED)
    new_peak = jnp.maximum(row_peak, jnp.max(scores, axis=-1))
    keep_factor = jnp.exp(row_peak - new_peak)
    weights = jnp.exp(scores - new_peak[:, :, None])
    row_total = row_total * keep_factor + jnp.sum(weights, axis=-1)
    accum_out = accum_out * keep_factor.T[:, :, None] + jnp.einsum(
        "htk,khd->thd",
        weights.astype(jnp.bfloat16),
        value_block,
        preferred_element_type=jnp.float32,
    )
    return (new_peak, row_total, accum_out)


def empty_state(head_count, width, local_tokens):
    return (
        jnp.full((head_count, local_tokens), MASKED, jnp.float32),
        jnp.zeros((head_count, local_tokens), jnp.float32),
        jnp.zeros((local_tokens, head_count, width), jnp.float32),
    )


def finish(carry_state):
    normalized = carry_state[2] / carry_state[1].T[:, :, None]
    return normalized.astype(jnp.bfloat16).reshape(normalized.shape[0], -1)


def project(latent_rows, weight):
    return jnp.dot(latent_rows, weight, preferred_element_type=jnp.float32).astype(jnp.bfloat16)


def body(
    query_wide,
    query_narrow,
    latent,
    rope_key,
    latent_norm_weight,
    broad_key_lift,
    broad_value_lift,
    slim_key_lift,
    slim_value_lift,
    out_wide,
    out_narrow,
    resid,
    ffn_gain,
    group_route,
    expert_pair,
    group_prob,
    expert_prob,
    gate_weight,
    up_weight,
    down_weight,
):
    local_tokens = latent.shape[0]
    offset = lax.axis_index("sp") * local_tokens
    query_pos = offset + jnp.arange(local_tokens, dtype=jnp.int32)
    angle_table = angles(query_pos, ROPE)
    latent_rows = rms_scale(latent, latent_norm_weight).astype(jnp.bfloat16)
    rot_key = rotary(rope_key.astype(jnp.float32), angle_table).astype(jnp.bfloat16)
    heads_wide = query_wide.shape[1] // (PLAIN_WIDTH_WIDE + ROPE)
    heads_narrow = query_narrow.shape[1] // (PLAIN_WIDTH_SLIM + ROPE)
    wide_query = split_query(query_wide, heads_wide, PLAIN_WIDTH_WIDE, angle_table)
    narrow_query = split_query(query_narrow, heads_narrow, PLAIN_WIDTH_SLIM, angle_table)

    def attend(carry_state, key_set, key_pos):
        key_w, value_w, key_n, value_n, rot_block = key_set
        block_rows = rot_block.shape[0]
        wide_state = group_step(
            carry_state[0],
            wide_query,
            key_w.reshape(block_rows, heads_wide, PLAIN_WIDTH_WIDE),
            value_w.reshape(block_rows, heads_wide, VALUE_WIDTH_WIDE),
            rot_block,
            key_pos,
            query_pos,
            (PLAIN_WIDTH_WIDE + ROPE) ** (-0.5),
        )
        narrow_state = group_step(
            carry_state[1],
            narrow_query,
            key_n.reshape(block_rows, heads_narrow, PLAIN_WIDTH_SLIM),
            value_n.reshape(block_rows, heads_narrow, VALUE_WIDTH_SLIM),
            rot_block,
            key_pos,
            query_pos,
            (PLAIN_WIDTH_SLIM + ROPE) ** (-0.5),
        )
        return (wide_state, narrow_state)

    start_state = (
        empty_state(heads_wide, VALUE_WIDTH_WIDE, local_tokens),
        empty_state(heads_narrow, VALUE_WIDTH_SLIM, local_tokens),
    )
    key_w = project(latent_rows, broad_key_lift)
    value_w = project(latent_rows, broad_value_lift)
    key_n = project(latent_rows, slim_key_lift)
    value_n = project(latent_rows, slim_value_lift)
    pieces = sent_together((key_w, value_w, key_n, value_n, rot_key), "sp", 0, 1)
    total_rows = pieces[0].shape[0]
    block_rows = math.gcd(total_rows, 1024)

    def visit_block(block_index, carry_inner):
        block_start = block_index * block_rows
        sliced = tuple(
            (lax.dynamic_slice_in_dim(piece, block_start, block_rows, 0) for piece in pieces)
        )
        key_pos = block_start + jnp.arange(block_rows, dtype=jnp.int32)

        def work_block(running):
            return attend(running, sliced, key_pos)

        return lax.cond(
            block_start > query_pos[-1], lambda unchanged: unchanged, work_block, carry_inner
        )

    final_state = lax.fori_loop(0, total_rows // block_rows, visit_block, start_state)
    att_wide = finish(final_state[0])
    att_narrow = finish(final_state[1])
    partial_value = jnp.dot(att_wide, out_wide, preferred_element_type=jnp.float32)
    partial_value = partial_value + jnp.dot(
        att_narrow, out_narrow, preferred_element_type=jnp.float32
    )
    model_width = resid.shape[1]
    tp_size = lax.axis_size("tp")
    quarter = model_width // tp_size
    col_start = lax.axis_index("tp") * quarter
    share = sum_at_owner(partial_value.astype(jnp.bfloat16), "tp", 1)
    resid_cols = lax.dynamic_slice_in_dim(resid, col_start, quarter, 1)
    stream_cols = (resid_cols.astype(jnp.float32) + share).astype(jnp.bfloat16)
    widened = stream_cols.astype(jnp.float32)
    square_total = of_everyone(jnp.sum(widened * widened, axis=1), "tp")
    gain_cols = lax.dynamic_slice_in_dim(ffn_gain, col_start, quarter, 0)
    normed_cols = (
        widened * lax.rsqrt(square_total[:, None] / model_width + EPSILON) * gain_cols[None, :]
    ).astype(jnp.bfloat16)
    groups = lax.axis_size("sp")
    capacity = 2 * local_tokens // groups
    share_of = group_prob[:, None] * expert_prob / jnp.sum(expert_prob, axis=1, keepdims=True)
    chosen = (expert_pair[:, :, None] == jnp.arange(EPG, dtype=jnp.int32)[None, None, :]).astype(
        jnp.float32
    )
    combine = jnp.sum(share_of[:, :, None] * chosen, axis=1).astype(jnp.bfloat16)
    member = (group_route[:, None] == jnp.arange(groups, dtype=jnp.int32)[None, :]).astype(
        jnp.int32
    )
    group_rank = jnp.sum(jnp.cumsum(member, axis=0) * member, axis=1) - 1
    slot_index = group_route * capacity + group_rank
    routed_weights = jnp.zeros((groups * capacity, EPG), jnp.bfloat16).at[slot_index].set(combine)
    routed_weights = routed_weights.reshape(groups, capacity, EPG)
    placed = (
        jnp.zeros((groups * capacity, normed_cols.shape[1]), jnp.bfloat16)
        .at[slot_index]
        .set(normed_cols)
    )
    joined = gathered_copies(
        lax.all_to_all(
            placed.reshape(groups, capacity, normed_cols.shape[1]),
            "sp",
            split_axis=0,
            concat_axis=0,
            tiled=True,
        ),
        "tp",
        2,
    )
    slot_count = joined.shape[0] * joined.shape[1]
    flat_rows = joined.reshape(slot_count, joined.shape[2])
    gate_act = jnp.einsum(
        "rd,edf->ref", flat_rows, gate_weight[0], preferred_element_type=jnp.float32
    )
    up_act = jnp.einsum("rd,edf->ref", flat_rows, up_weight[0], preferred_element_type=jnp.float32)
    scaled = (
        lax.all_to_all(routed_weights, "sp", split_axis=0, concat_axis=0, tiled=True)
        .reshape(slot_count, EPG)
        .astype(jnp.float32)[:, :, None]
    )
    hidden = (jax.nn.silu(gate_act) * up_act * scaled).astype(jnp.bfloat16)
    partials = jnp.einsum("ref,efd->rd", hidden, down_weight[0], preferred_element_type=jnp.float32)
    partials = partials.reshape(joined.shape)
    summed_rows = sum_at_owner(partials.astype(jnp.bfloat16), "tp", 2).astype(jnp.bfloat16)
    returned_rows = lax.all_to_all(summed_rows, "sp", split_axis=0, concat_axis=0, tiled=True)
    moe_rows = returned_rows.reshape(groups * capacity, quarter)[slot_index]
    return (stream_cols.astype(jnp.float32) + moe_rows.astype(jnp.float32)).astype(jnp.bfloat16)


def solution(mesh):
    placed = (
        P("sp", "tp"),
        P("sp", "tp"),
        P("sp", None),
        P("sp", None),
        P(),
        P(None, "tp"),
        P(None, "tp"),
        P(None, "tp"),
        P(None, "tp"),
        P("tp", None),
        P("tp", None),
        P("sp", None),
        P(),
        P("sp"),
        P("sp", None),
        P("sp"),
        P("sp", None),
        P("sp", None, None, "tp"),
        P("sp", None, None, "tp"),
        P("sp", None, "tp", None),
    )
    return jax.shard_map(body, mesh=mesh, in_specs=placed, out_specs=P("sp", "tp"), check_vma=False)
```

profile of v0, /device:TPU:1, one launch (start us, length us, event | category | flops | bytes accessed | tf_op | source)
XLA Modules:
  0.0 333.1 jit_solution(4039350094087601190)
XLA Ops:
  6.6 1.2 fusion.40
  7.8 1.3 convolution_convert_fusion.1
  9.1 1.3 convolution_convert_fusion
  10.3 1.2 convolution_convert_fusion.3
  11.6 1.2 convolution_convert_fusion.2
  12.8 0.7 convert_element_type.126
  13.9 0.8 concatenate.14
  15.7 97.5 %all-gather.2.cloned.1.call-done = bf16[8192,832]{1,0:T(8,128)(2,1)} async-done(((bf16[128,832]{1,0:T(8,128)(2,1)}), bf16[8192,832]{1,0:T(8,128)(2,1)}) %all-gather.2.cloned.1.call-update) | async-done | bytes 13631504 | tf_op jit(solution)/shard_map/all_gather | solution.py:24
  113.2 6.0 %fusion.64 = (bf16[8192,256]{1,0:T(8,128)(2,1)}, bf16[8192,256]{1,0:T(8,128)(2,1)}) fusion(bf16[8192,832]{1,0:T(8,128)(2,1)} %all-gather.2.cloned.1.call-done), kind=kLoop, calls=%fused_computation.112 | loop fusion | bytes 16777216 | tf_op jit(solution)/shard_map/split | solution.py:25
  119.2 6.4 %copy.184 = bf16[8192,256]{0,1:T(8,128)(2,1)} copy(bf16[8192,256]{1,0:T(8,128)(2,1)} %get-tuple-element.691) | data formatting | bytes 8388608 | tf_op jit(solution)/shard_map/while | solution.py:220
  125.6 3.0 split.21
  128.6 1.9 copy.186
  130.5 6.4 %copy.187 = bf16[8192,256]{0,1:T(8,128)(2,1)} copy(bf16[8192,256]{1,0:T(8,128)(2,1)} %get-tuple-element.690) | data formatting | bytes 8388608 | tf_op jit(solution)/shard_map/while | solution.py:220
  136.9 4.5 %fusion.63 = (bf16[8192,128]{1,0:T(8,128)(2,1)}, bf16[8192,128]{1,0:T(8,128)(2,1)}) fusion(bf16[8192,832]{1,0:T(8,128)(2,1)} %all-gather.2.cloned.1.call-done), kind=kLoop, calls=%fused_computation.111 | loop fusion | bytes 8388608 | tf_op jit(solution)/shard_map/split | solution.py:25
  141.4 4.1 %copy.188 = bf16[8192,128]{0,1:T(8,128)(2,1)} copy(bf16[8192,128]{1,0:T(8,128)(2,1)} %get-tuple-element.689) | data formatting | bytes 4194304 | tf_op jit(solution)/shard_map/while | solution.py:220
  145.5 4.1 %copy.189 = bf16[8192,128]{0,1:T(8,128)(2,1)} copy(bf16[8192,128]{1,0:T(8,128)(2,1)} %get-tuple-element.688) | data formatting | bytes 4194304 | tf_op jit(solution)/shard_map/while | solution.py:220
  149.7 15.8 %while.23 = (s32[]{:T(128)}, f32[2,128]{1,0:T(2,128)S(1)}, f32[2,128]{1,0:T(2,128)S(1)}, f32[128,2,128]{2,0,1:T(8,128)S(1)}, f32[2,128]{1,0:T(2,128)S(1)}, /*ind...) while((s32[]{:T(128)}, f32[2,128]{1,0:T(2,128)S(1)}, ...), condition=%wide.region_8.9_spmd, body=%wide.region_1.8_spmd.sunk | while | flops 272861696 | bytes 16466941 | solution.py:220
  149.7 0.6 slice.75
  150.9 5.2 %conditional.2 = (f32[2,128]{1,0:T(2,128)S(1)}, f32[2,128]{1,0:T(2,128)S(1)}, f32[128,2,128]{2,0,1:T(8,128)S(1)}, f32[2,128]{1,0:T(2,128)S(1)}, f32[2,128]{1,0:T(2,128)S(1)}, /*index=5*/f32[128,2,64]{0,2,1:T(8,128)S(1)}) conditional(s32[]{:T(128)} %convert_element_type.204, (s32[128]{0:T(128)S(1)}, s32[]{:T(128)}, s32[1024]{0:T(1024)S(1)}, ...), branch_computations={%region_2.6_spmd, %region_7.7_spmd} | conditional | flops 272861696 | bytes 16458342 | solution.py:216
  150.9 1.3 constant_dynamic-slice_fusion.2
  152.2 0.3 convolution_bitcast_fusion
  152.8 0.4 fusion.61
  153.4 0.4 fusion.6
  153.8 1.1 constant_dynamic-slice_fusion
  154.8 0.4 convolution_bitcast_fusion.2
  155.2 0.4 fusion.62
  155.8 0.3 fusion.7
  156.2 0.6 slice.75
  157.5 0.6 slice.75
  158.8 0.6 slice.75
  160.2 0.6 slice.75
  161.5 0.6 slice.75
  162.8 0.6 slice.75
  164.2 0.6 slice.75
  165.6 1.6 fusion.65
  167.3 0.3 fusion.25
  167.6 0.8 copy.220
  168.4 4.0 %all-to-all-start = ((bf16[4,128,512]{2,1,0:T(8,128)(2,1)}), bf16[4,128,512]{2,1,0:T(8,128)(2,1)S(1)}, u32[]{:S(2)}, u32[]{:S(2)}) async-start(bf16[4,128,512]{2,1,0:T(8,128)(2,1)} %bitcast.110), calls=%async_computation | async-start | bytes 1048576 | tf_op jit(solution)/shard_map/all_to_all | solution.py:35
  172.5 9.0 %all-to-all-done = bf16[4,128,512]{2,1,0:T(8,128)(2,1)S(1)} async-done(((bf16[4,128,512]{2,1,0:T(8,128)(2,1)}), bf16[4,128,512]{2,1,0:T(8,128)(2,1)S(1)}, u32[]{:S(2)}, u32[]{:S(2)}) %all-to-all-start) | async-done | bytes 524320 | tf_op jit(solution)/shard_map/all_to_all | solution.py:35
  181.5 1.0 fusion.43
  182.6 0.6 broadcast_in_dim.51
  183.2 3.2 all-to-all-start.1
  186.4 0.8 dynamic_slice.72
  187.3 0.9 scatter_custom_fusion.1
  188.3 1.1 copy.196
  189.4 1.1 all-to-all-done.1
  190.5 42.6 %all-to-all-start.4 = ((bf16[64,4,4]{1,2,0:T(4,128)(2,1)}), bf16[64,4,4]{1,2,0:T(4,128)(2,1)S(1)}, u32[]{:S(2)}, u32[]{:S(2)}) async-start(bf16[64,4,4]{1,2,0:T(4,128)(2,1)} %copy.196), calls=%async_computation.4 | async-start | bytes 131072 | tf_op jit(solution)/shard_map/all_to_all | solution.py:277
  233.1 1.2 scatter_custom_fusion
  234.4 8.8 %all-to-all-done.4 = bf16[64,4,4]{1,2,0:T(4,128)(2,1)S(1)} async-done(((bf16[64,4,4]{1,2,0:T(4,128)(2,1)}), bf16[64,4,4]{1,2,0:T(4,128)(2,1)S(1)}, u32[]{:S(2)}, u32[]{:S(2)}) %all-to-all-start.4) | async-done | bytes 2080 | tf_op jit(solution)/shard_map/all_to_all | solution.py:277
  243.2 16.8 %all_to_all.36 = bf16[64,4,512]{2,1,0:T(4,128)(2,1)S(1)} all-to-all(bf16[64,4,512]{2,1,0:T(4,128)(2,1)S(1)} %reshape.188), channel_id=1, replica_groups=mesh['sp'=64,'tp'=4] {'sp'}, dimensions={0} | all-to-all | bytes 524288 | tf_op jit(solution)/shard_map/all_to_all | solution.py:260
  259.9 1.3 broadcast_in_dim.52
  261.2 3.7 %all-to-all-start.3 = ((bf16[4,64,4,512]{3,2,1,0:T(4,128)(2,1)}), bf16[4,64,4,512]{3,2,1,0:T(4,128)(2,1)S(1)}, u32[]{:S(2)}, u32[]{:S(2)}) async-start(bf16[4,64,4,512]{3,2,1,0:T(4,128)(2,1)} %broadcast_in_dim.52), calls=%async_computation.3 | async-start | bytes 2097152 | tf_op jit(solution)/shard_map/all_to_all | solution.py:41
  265.3 14.3 %all-to-all-done.3 = bf16[4,64,4,512]{3,2,1,0:T(4,128)(2,1)S(1)} async-done(((bf16[4,64,4,512]{3,2,1,0:T(4,128)(2,1)}), bf16[4,64,4,512]{3,2,1,0:T(4,128)(2,1)S(1)}, u32[]{:S(2)}, u32[]{:S(2)}) %all-to-all-start.3) | async-done | bytes 1048608 | tf_op jit(solution)/shard_map/all_to_all | solution.py:41
  279.6 2.3 copy.193
  282.0 1.8 reshape.221
  283.8 2.4 fusion.29
  286.2 0.7 fusion.37
  287.0 0.7 fusion.24
  287.8 16.5 %all_to_all.37 = bf16[4,64,4,512]{3,1,2,0:T(8,128)(2,1)S(1)} all-to-all(bf16[4,64,4,512]{3,1,2,0:T(8,128)(2,1)S(1)} %bitcast.118), channel_id=1, replica_groups=mesh['sp'=64,'tp'=4] {'tp'}, dimensions={0} | all-to-all | bytes 2097152 | tf_op jit(solution)/shard_map/all_to_all | solution.py:35
  304.6 0.9 copy.202
  305.5 6.1 %all-to-all-start.6 = ((bf16[64,4,512]{2,1,0:T(4,128)(2,1)}), bf16[64,4,512]{2,1,0:T(4,128)(2,1)S(1)}, u32[]{:S(2)}, u32[]{:S(2)}) async-start(bf16[64,4,512]{2,1,0:T(4,128)(2,1)} %copy.202), calls=%async_computation.6 | async-start | bytes 524288 | tf_op jit(solution)/shard_map/all_to_all | solution.py:285
  311.6 13.1 %all-to-all-done.6 = bf16[64,4,512]{2,1,0:T(4,128)(2,1)S(1)} async-done(((bf16[64,4,512]{2,1,0:T(4,128)(2,1)}), bf16[64,4,512]{2,1,0:T(4,128)(2,1)S(1)}, u32[]{:S(2)}, u32[]{:S(2)}) %all-to-all-start.6) | async-done | bytes 262176 | tf_op jit(solution)/shard_map/all_to_all | solution.py:285
  324.8 0.8 gather_fusion
  325.6 0.7 fusion.46
  (120 shorter events, 3.6 us)
Async XLA Ops:
  6.5 280.5 %copy-start = (bf16[1,4,128,2048]{3,2,1,0:T(8,128)(2,1)S(1)}, bf16[1,4,128,2048]{3,2,1,0:T(8,128)(2,1)}, u32[]{:S(2)}) copy-start(bf16[1,4,128,2048]{3,2,1,0:T(8,128)(2,1)} %param.43) | copy-start | bytes 6291460
  6.5 8.2 %copy-start.2 = (bf16[128,384]{1,0:T(8,128)(2,1)S(1)}, bf16[128,384]{1,0:T(8,128)(2,1)}, u32[]{:S(2)}) copy-start(bf16[128,384]{1,0:T(8,128)(2,1)} %param.24) | copy-start | bytes 294916
  6.5 8.5 %copy-start.3 = (bf16[128,256]{1,0:T(8,128)(2,1)S(1)}, bf16[128,256]{1,0:T(8,128)(2,1)}, u32[]{:S(2)}) copy-start(bf16[128,256]{1,0:T(8,128)(2,1)} %param.25) | copy-start | bytes 196612
  6.5 8.6 %copy-start.5 = (s32[128]{0:T(128)S(1)}, s32[128]{0:T(128)}, u32[]{:S(2)}) copy-start(s32[128]{0:T(128)} %param.37) | copy-start | bytes 1540
  6.5 8.9 %copy-start.4 = (f32[128,2]{0,1:T(2,128)S(1)}, f32[128,2]{0,1:T(2,128)}, u32[]{:S(2)}) copy-start(f32[128,2]{0,1:T(2,128)} %param.40) | copy-start | bytes 3076
  6.5 106.7 %all-gather.2.cloned.1.call-start = ((), (), s32[]{:S(2)}) async-start(), calls=%async_computation.7 | async-start | bytes 14909440 | tf_op jit(solution)/shard_map/all_gather | solution.py:24
  165.5 1.8 copy-start.1
  167.2 5.2 %copy-start.9 = (f32[128]{0:T(128)S(1)}, f32[128]{0:T(128)}, u32[]{:S(2)}) copy-start(f32[128]{0:T(128)} %param.39) | copy-start | bytes 1540
  167.6 18.8 %copy-start.6 = (s32[128,2]{0,1:T(2,128)S(1)}, s32[128,2]{0,1:T(2,128)}, u32[]{:S(2)}) copy-start(s32[128,2]{0,1:T(2,128)} %param.38) | copy-start | bytes 3076
  168.4 13.0 %all-to-all-start = ((bf16[4,128,512]{2,1,0:T(8,128)(2,1)}), bf16[4,128,512]{2,1,0:T(8,128)(2,1)S(1)}, u32[]{:S(2)}, u32[]{:S(2)}) async-start(bf16[4,128,512]{2,1,0:T(8,128)(2,1)} %bitcast.110), calls=%async_computation | async-start | bytes 1048576 | tf_op jit(solution)/shard_map/all_to_all | solution.py:35
  172.4 88.8 %copy-start.7 = (s32[128]{0:T(128)}, s32[128]{0:T(128)S(1)}, u32[]{:S(2)}) copy-start(s32[128]{0:T(128)S(1)} %compare_select_fusion) | copy-start | bytes 1540
  183.2 7.4 %all-to-all-start.1 = ((f32[4,1,128]{2,1,0:T(1,128)}), f32[4,1,128]{2,1,0:T(1,128)S(1)}, u32[]{:S(2)}, u32[]{:S(2)}) async-start(f32[4,1,128]{2,1,0:T(1,128)} %broadcast_in_dim.51), calls=%async_computation.1 | async-start | bytes 4096 | tf_op jit(solution)/shard_map/all_to_all | solution.py:41
  190.5 52.7 %all-to-all-start.4 = ((bf16[64,4,4]{1,2,0:T(4,128)(2,1)}), bf16[64,4,4]{1,2,0:T(4,128)(2,1)S(1)}, u32[]{:S(2)}, u32[]{:S(2)}) async-start(bf16[64,4,4]{1,2,0:T(4,128)(2,1)} %copy.196), calls=%async_computation.4 | async-start | bytes 131072 | tf_op jit(solution)/shard_map/all_to_all | solution.py:277
  261.2 18.4 %all-to-all-start.3 = ((bf16[4,64,4,512]{3,2,1,0:T(4,128)(2,1)}), bf16[4,64,4,512]{3,2,1,0:T(4,128)(2,1)S(1)}, u32[]{:S(2)}, u32[]{:S(2)}) async-start(bf16[4,64,4,512]{3,2,1,0:T(4,128)(2,1)} %broadcast_in_dim.52), calls=%async_computation.3 | async-start | bytes 2097152 | tf_op jit(solution)/shard_map/all_to_all | solution.py:41
  283.8 2.5 copy-start.10
  287.8 23.8 %copy-start.8 = (s32[128]{0:T(128)S(1)}, s32[128]{0:T(128)}, u32[]{:S(2)}) copy-start(s32[128]{0:T(128)} %copy-done.7) | copy-start | bytes 1540
  305.5 19.2 %all-to-all-start.6 = ((bf16[64,4,512]{2,1,0:T(4,128)(2,1)}), bf16[64,4,512]{2,1,0:T(4,128)(2,1)S(1)}, u32[]{:S(2)}, u32[]{:S(2)}) async-start(bf16[64,4,512]{2,1,0:T(4,128)(2,1)} %copy.202), calls=%async_computation.6 | async-start | bytes 524288 | tf_op jit(solution)/shard_map/all_to_all | solution.py:285
Sparse Core Ops, SparseCore 0:
  14.9 98.3 all-gather.1
where the time goes:
time: 335 us; the launch traced here: 333 us
  waiting for transfers between devices  144 us (43%)
  starting transfers between devices  59.7 us (18%)
  local copies, waits for them, and re-layouts  57.4 us (17%)
  blocking collectives  33.3 us (10%)
  between operations  13.9 us (4%)
  matrix products  12.9 us (4%)
  other arithmetic  6.42 us (2%)
  loops' own time  5.7 us (2%)
    all_gather x1, waiting for transfers between devices, sent_together(): result = lax.all_gather(both, axis, axis=dim, tiled=True)  97.5 us
    all_to_all x1, starting transfers between devices, body(): lax.all_to_all(routed_weights, 'sp', split_axis=0, concat_axis=0, tiled=T...  42.6 us
    while x7, local copies, waits for them, and re-layouts, body(): lax.fori_loop(0, total_rows // block_rows, visit_block, start_state)  23 us
    all_to_all x1, blocking collectives, body(): lax.all_to_all(placed.reshape(groups, capacity, normed_cols.shape[1]), 's...  16.8 us
    all_to_all x1, blocking collectives, sum_at_owner(): lax.all_to_all(blocks, axis, split_axis=0, concat_axis=0, tiled=True)  16.5 us
    all_to_all x2, waiting for transfers between devices, sent_to_all(): return lax.all_to_all(copies, axis, split_axis=0, concat_axis=0, tiled=True)  15.5 us
    split x3, local copies, waits for them, and re-layouts, sent_together(): jnp.split(result, [sum(widths[:k]) for k in range(1, len(widths))], axis=...  13.6 us
    all_to_all x1, waiting for transfers between devices, body(): lax.all_to_all(summed_rows, 'sp', split_axis=0, concat_axis=0, tiled=True)  13.1 us
  transfers between devices with their start and end apart: 6, of which 6 were waited for; matrix products, arithmetic and copies ran while one was open for 2% of the time, Pallas kernels for 0%

commit v1 on v0

v1 whole, which is shorter than its diff:
```python
import functools

import jax
import jax.numpy as jnp
from jax import lax
from jax.experimental import pallas as pl
from jax.experimental.pallas import tpu as pltpu
from jax.sharding import PartitionSpec as P

PLAIN_WIDTH_WIDE = 128
PLAIN_WIDTH_SLIM = 64
ROPE = 64
VALUE_WIDTH_WIDE = 128
VALUE_WIDTH_SLIM = 64
EPG = 4


ROPE_BASE = 10000.0
EPSILON = 1e-06
MASKED = -1e30


def in_blocks(x, dim, peers):
    before, after = (x.shape[:dim], x.shape[dim + 1 :])
    return jnp.moveaxis(x.reshape(*before, peers, -1, *after), dim, 0)


def sum_at_owner(x, axis, dim):
    blocks = in_blocks(x, dim, lax.axis_size(axis))
    arrived = lax.all_to_all(blocks, axis, split_axis=0, concat_axis=0, tiled=True)
    return arrived.astype(jnp.float32).sum(axis=0)


def sent_to_all(x, axis):
    copies = jnp.broadcast_to(x, (lax.axis_size(axis), *x.shape))
    return lax.all_to_all(copies, axis, split_axis=0, concat_axis=0, tiled=True)


def of_everyone(x, axis):
    everything = sent_to_all(x, axis)
    return jnp.sum(everything, axis=0)


def joined_along(blocks, dim):
    blocks = jnp.moveaxis(blocks, 0, dim)
    shape = blocks.shape
    return blocks.reshape(*shape[:dim], shape[dim] * shape[dim + 1], *shape[dim + 2 :])


def gathered_copies(x, axis, dim):
    blocks = sent_to_all(x, axis)
    return joined_along(blocks, dim)


def rms_scale(values, gain_row):
    widened = values.astype(jnp.float32)
    return (
        widened
        * lax.rsqrt(jnp.mean(widened * widened, axis=-1, keepdims=True) + EPSILON)
        * gain_row
    )


def angles(positions, width):
    frequency = 1.0 / ROPE_BASE ** (jnp.arange(0, width, 2).astype(jnp.float32) / width)
    return positions.astype(jnp.float32)[:, None] * frequency[None, :]


MESH = pl.DeviceIdType.MESH
LOG2E = 1.4426950408889634
Z = 8
XC = 8
BLOCK = 128
HEAD_ROWS = ((0, 128), (128, 256), (256, 320), (320, 384))
HEAD_QUERY = ((0, 256), (128, 384), (384, 512), (512, 640))
HEAD_KEY = ((0, 256), (256, 512), (512, 640), (640, 768))
HEAD_SCALE = (192**-0.5 * LOG2E, 192**-0.5 * LOG2E, 128**-0.5 * LOG2E, 128**-0.5 * LOG2E)


def nt(a, b):
    return lax.dot_general(a, b, (((1,), (1,)), ((), ())), preferred_element_type=jnp.float32)


def nn(a, b):
    return lax.dot_general(a, b, (((1,), (0,)), ((), ())), preferred_element_type=jnp.float32)


def remote(src, dst, send_sem, recv_sem, sp):
    return pltpu.make_async_remote_copy(
        src_ref=src,
        dst_ref=dst,
        send_sem=send_sem,
        recv_sem=recv_sem,
        device_id={"sp": sp},
        device_id_type=MESH,
    )


def attention_kernel(
    qw_ref, qn_ref, latent_ref, rope_ref, gain_ref, wbk_ref, wbv_ref, wsk_ref, wsv_ref, cos_ref, sin_ref,
    out_ref,
    q_all, lat_all, keys, values, acc, peak, total, o_send, o_recv, s_send, s_recv,
    q_ssem, q_rsem, up_ssem, up_rsem, dn_ssem, dn_rsem, o_ssem, o_rsem, t_ssem, t_rsem,
):
    sp = lax.axis_index("sp")
    z = sp // XC
    xc = lax.rem(sp, XC)
    core = lax.rem(xc, 2)
    base = z * XC
    sibling = base + xc + 1 - 2 * core
    above = lax.rem(sp + XC, Z * XC)
    below = lax.rem(sp + (Z - 1) * XC, Z * XC)

    barrier = pltpu.get_barrier_semaphore()
    for d in range(1, XC):
        pl.semaphore_signal(barrier, inc=1, device_id={"sp": base + lax.rem(xc + d, XC)}, device_id_type=MESH)
    for peer in (above, below):
        pl.semaphore_signal(barrier, inc=1, device_id={"sp": peer}, device_id_type=MESH)

    lane = lax.broadcasted_iota(jnp.int32, (BLOCK, 128), 1)
    low = lane < 64
    first = lax.rem(lane, 64) < 32
    cos = cos_ref[...]
    sin = sin_ref[...]

    def turned(x):
        swapped = jnp.where(first, pltpu.roll(x, 96, 1), pltpu.roll(x, 32, 1))
        return x * cos + swapped * sin

    q_all[xc, :, 0:128] = qw_ref[:, 0:128]
    middle = qw_ref[:, 128:256].astype(jnp.float32)
    last = qw_ref[:, 256:384].astype(jnp.float32)
    q_all[xc, :, 128:256] = turned(jnp.where(low, middle, last)).astype(jnp.bfloat16)
    q_all[xc, :, 256:384] = pltpu.roll(jnp.where(low, last, middle), 64, 1).astype(jnp.bfloat16)
    for k in range(2):
        x = qn_ref[:, k * 128 : (k + 1) * 128].astype(jnp.float32)
        q_all[xc, :, 384 + k * 128 : 512 + k * 128] = jnp.where(low, x, turned(x)).astype(jnp.bfloat16)
    x = latent_ref[...].astype(jnp.float32)
    x = x * lax.rsqrt(jnp.mean(x * x, axis=1, keepdims=True) + EPSILON) * gain_ref[...]
    lat_all[z, :, 0:512] = x.astype(jnp.bfloat16)
    lat_all[z, :, 512:640] = turned(rope_ref[...].astype(jnp.float32)).astype(jnp.bfloat16)

    pl.semaphore_wait(barrier, XC + 1)

    def q_direct(d):
        return remote(
            q_all.at[xc], q_all.at[xc], q_ssem.at[d], q_rsem.at[d], base + lax.rem(xc + 2 * d, XC)
        )

    def q_sibling():
        return remote(q_all.at[xc], q_all.at[xc], q_ssem.at[0], q_rsem.at[0], sibling)

    def q_forward(d):
        slot = lax.rem(xc + 2 * (4 - d), XC)
        return remote(q_all.at[slot], q_all.at[slot], q_ssem.at[3 + d], q_rsem.at[3 + d], sibling)

    def up_copy(s):
        slot = lax.rem(z - s + 1 + Z, Z)
        return remote(lat_all.at[slot], lat_all.at[slot], up_ssem.at[s], up_rsem.at[s], above)

    def dn_copy(s):
        slot = lax.rem(z + s - 1, Z)
        return remote(lat_all.at[slot], lat_all.at[slot], dn_ssem.at[s], dn_rsem.at[s], below)

    def up_sends(s):
        return (s <= 4) & (z - s + 1 >= 0) & (z < Z - 1)

    def up_comes(s):
        return z - s >= 0

    def dn_sends(s):
        return (s <= 3) & (lax.rem(z + s - 1, Z) <= 2)

    def dn_comes(s):
        return (s <= 3) & (lax.rem(z + s, Z) <= 2)

    def start_step(s):
        @pl.when(up_sends(s))
        def _():
            up_copy(s).start()

        @pl.when(dn_sends(s))
        def _():
            dn_copy(s).start()

    def arrive_step(s):
        @pl.when(up_comes(s))
        def _():
            up_copy(s).wait_recv()

        @pl.when(dn_comes(s))
        def _():
            dn_copy(s).wait_recv()

    start_step(1)
    q_sibling().start()
    for d in range(1, 4):
        q_direct(d).start()

    peak[...] = jnp.full(peak.shape, MASKED, jnp.float32)
    total[...] = jnp.zeros(total.shape, jnp.float32)
    acc[...] = jnp.zeros(acc.shape, jnp.float32)

    def project(slot):
        rows = lat_all[slot, :, 0:512]
        rot = lat_all[slot, :, 512:640]
        wide = nn(rows, wbk_ref[...]).astype(jnp.bfloat16)
        zero = jnp.zeros_like(rot)
        keys[:, 0:128] = wide[:, 0:128]
        keys[:, 128:256] = jnp.where(low, rot, zero)
        keys[:, 256:384] = jnp.where(low, zero, rot)
        keys[:, 384:512] = wide[:, 128:256]
        slim = nn(rows, wsk_ref[...])
        keys[:, 512:640] = jnp.where(low, slim.astype(jnp.bfloat16), rot)
        keys[:, 640:768] = jnp.where(low, pltpu.roll(slim, 64, 1).astype(jnp.bfloat16), rot)
        values[0:256, :] = jnp.transpose(nn(rows, wbv_ref[...])).astype(jnp.bfloat16)
        values[256:384, :] = jnp.transpose(nn(rows, wsv_ref[...])).astype(jnp.bfloat16)

    def attend(slot, own):
        project(slot)

        def chunk(c, carry):
            if own:
                key_pos = xc * BLOCK + lax.broadcasted_iota(jnp.int32, (BLOCK, 256), 0)
                query_pos = c * 256 + lax.broadcasted_iota(jnp.int32, (BLOCK, 256), 1)
                seen = key_pos <= query_pos
            for h in range(4):
                ql, qh = HEAD_QUERY[h]
                kl, kh = HEAD_KEY[h]
                lo, hi = HEAD_ROWS[h]
                q = q_all[pl.ds(2 * c, 2), :, ql:qh].reshape(256, qh - ql)
                scores = nt(keys[:, kl:kh], q) * HEAD_SCALE[h]
                if own:
                    scores = jnp.where(seen, scores, MASKED)
                before = peak[c, h : h + 1, :]
                top = jnp.maximum(before, jnp.max(scores, axis=0, keepdims=True))
                keep = jnp.exp2(before - top)
                weights = jnp.exp2(scores - top)
                peak[c, h : h + 1, :] = top
                total[c, h : h + 1, :] = total[c, h : h + 1, :] * keep + jnp.sum(weights, axis=0, keepdims=True)
                acc[c, lo:hi, :] = acc[c, lo:hi, :] * keep + nn(values[lo:hi, :], weights.astype(jnp.bfloat16))
            return carry

        lax.fori_loop(0, 4, chunk, 0)

    arrive_step(1)
    start_step(2)
    for d in range(1, 4):
        q_direct(d).wait_recv()
        q_forward(d).start()
    q_sibling().wait_recv()
    for d in range(1, 4):
        q_forward(d).wait_recv()
    attend(z, True)

    def step(s, carry):
        @pl.when(s > 1)
        def _():
            arrive_step(s)
            start_step(s + 1)

        @pl.when(z - s >= 0)
        def _():
            attend(z - s, False)

        @pl.when((s <= 3) & (z + s >= Z))
        def _():
            attend(z + s - Z, False)

        return carry

    lax.fori_loop(1, 5, step, 0)

    for j in range(XC):
        c, lanes = j // 2, slice((j % 2) * 128, (j % 2) * 128 + 128)
        for h in range(4):
            lo, hi = HEAD_ROWS[h]
            o_send[j, lo:hi, :] = (acc[c, lo:hi, lanes] / total[c, h : h + 1, lanes]).astype(jnp.bfloat16)
            s_send[j, h : h + 1, :] = peak[c, h : h + 1, lanes]
            s_send[j, 4 + h : 5 + h, :] = total[c, h : h + 1, lanes]

    def o_copy(d):
        j = lax.rem(xc + d, XC)
        return remote(o_send.at[j], o_recv.at[xc], o_ssem.at[d], o_rsem.at[d], base + j)

    def s_copy(d):
        j = lax.rem(xc + d, XC)
        return remote(s_send.at[j], s_recv.at[xc], t_ssem.at[d], t_rsem.at[d], base + j)

    for d in range(1, XC):
        s_copy(d).start()
        o_copy(d).start()
    o_recv[xc] = o_send[xc]
    s_recv[xc] = s_send[xc]
    for d in range(1, XC):
        s_copy(d).wait_recv()
        o_copy(d).wait_recv()
    for h in range(4):
        lo, hi = HEAD_ROWS[h]
        tops = [s_recv[j, h : h + 1, :] for j in range(XC)]
        top = functools.reduce(jnp.maximum, tops)
        shares = [jnp.exp2(tops[j] - top) * s_recv[j, 4 + h : 5 + h, :] for j in range(XC)]
        whole = functools.reduce(jnp.add, shares)
        mixed = functools.reduce(
            jnp.add, [o_recv[j, lo:hi, :].astype(jnp.float32) * (shares[j] / whole) for j in range(XC)]
        )
        out_ref[lo:hi, :] = mixed.astype(jnp.bfloat16)

    q_sibling().wait_send()
    for d in range(1, 4):
        q_direct(d).wait_send()
        q_forward(d).wait_send()
    for s in range(1, 5):

        @pl.when(up_sends(s))
        def _(s=s):
            up_copy(s).wait_send()

    for s in range(1, 4):

        @pl.when(dn_sends(s))
        def _(s=s):
            dn_copy(s).wait_send()

    for d in range(1, XC):
        s_copy(d).wait_send()
        o_copy(d).wait_send()


def attention(query_wide, query_narrow, latent, rope_key, gain, wbk, wbv, wsk, wsv):
    position = lax.axis_index("sp") * BLOCK + jnp.arange(BLOCK, dtype=jnp.int32)
    angle = angles(position, ROPE)
    cos = jnp.tile(jnp.cos(angle), (1, 4))
    sin = jnp.sin(angle)
    sin = jnp.concatenate([-sin, sin, -sin, sin], axis=1)
    vmem = pl.BlockSpec(memory_space=pltpu.VMEM)
    bf16, f32, dma = jnp.bfloat16, jnp.float32, pltpu.SemaphoreType.DMA
    return pl.pallas_call(
        attention_kernel,
        out_shape=jax.ShapeDtypeStruct((384, BLOCK), bf16),
        in_specs=[vmem] * 11,
        out_specs=vmem,
        scratch_shapes=[
            pltpu.VMEM((XC, BLOCK, 640), bf16),
            pltpu.VMEM((Z, BLOCK, 640), bf16),
            pltpu.VMEM((BLOCK, 768), bf16),
            pltpu.VMEM((384, BLOCK), bf16),
            pltpu.VMEM((4, 384, 256), f32),
            pltpu.VMEM((4, 8, 256), f32),
            pltpu.VMEM((4, 8, 256), f32),
            pltpu.VMEM((XC, 384, BLOCK), bf16),
            pltpu.VMEM((XC, 384, BLOCK), bf16),
            pltpu.VMEM((XC, 8, BLOCK), f32),
            pltpu.VMEM((XC, 8, BLOCK), f32),
            dma((7,)), dma((7,)), dma((6,)), dma((6,)), dma((6,)), dma((6,)),
            dma((8,)), dma((8,)), dma((8,)), dma((8,)),
        ],
        compiler_params=pltpu.CompilerParams(collective_id=0, has_side_effects=True),
        name="attention",
    )(
        query_wide, query_narrow, latent, jnp.concatenate([rope_key, rope_key], axis=1), gain[None, :],
        wbk, wbv, wsk, wsv, cos, sin,
    )


def body(
    query_wide,
    query_narrow,
    latent,
    rope_key,
    latent_norm_weight,
    broad_key_lift,
    broad_value_lift,
    slim_key_lift,
    slim_value_lift,
    out_wide,
    out_narrow,
    resid,
    ffn_gain,
    group_route,
    expert_pair,
    group_prob,
    expert_prob,
    gate_weight,
    up_weight,
    down_weight,
):
    local_tokens = latent.shape[0]
    att = attention(
        query_wide, query_narrow, latent, rope_key, latent_norm_weight,
        broad_key_lift, broad_value_lift, slim_key_lift, slim_value_lift,
    )
    partial_value = lax.dot_general(
        att, jnp.concatenate([out_wide, out_narrow], axis=0), (((0,), (0,)), ((), ())),
        preferred_element_type=jnp.float32,
    )
    model_width = resid.shape[1]
    tp_size = lax.axis_size("tp")
    quarter = model_width // tp_size
    col_start = lax.axis_index("tp") * quarter
    share = sum_at_owner(partial_value.astype(jnp.bfloat16), "tp", 1)
    resid_cols = lax.dynamic_slice_in_dim(resid, col_start, quarter, 1)
    stream_cols = (resid_cols.astype(jnp.float32) + share).astype(jnp.bfloat16)
    widened = stream_cols.astype(jnp.float32)
    square_total = of_everyone(jnp.sum(widened * widened, axis=1), "tp")
    gain_cols = lax.dynamic_slice_in_dim(ffn_gain, col_start, quarter, 0)
    normed_cols = (
        widened * lax.rsqrt(square_total[:, None] / model_width + EPSILON) * gain_cols[None, :]
    ).astype(jnp.bfloat16)
    groups = lax.axis_size("sp")
    capacity = 2 * local_tokens // groups
    share_of = group_prob[:, None] * expert_prob / jnp.sum(expert_prob, axis=1, keepdims=True)
    chosen = (expert_pair[:, :, None] == jnp.arange(EPG, dtype=jnp.int32)[None, None, :]).astype(
        jnp.float32
    )
    combine = jnp.sum(share_of[:, :, None] * chosen, axis=1).astype(jnp.bfloat16)
    member = (group_route[:, None] == jnp.arange(groups, dtype=jnp.int32)[None, :]).astype(
        jnp.int32
    )
    group_rank = jnp.sum(jnp.cumsum(member, axis=0) * member, axis=1) - 1
    slot_index = group_route * capacity + group_rank
    routed_weights = jnp.zeros((groups * capacity, EPG), jnp.bfloat16).at[slot_index].set(combine)
    routed_weights = routed_weights.reshape(groups, capacity, EPG)
    placed = (
        jnp.zeros((groups * capacity, normed_cols.shape[1]), jnp.bfloat16)
        .at[slot_index]
        .set(normed_cols)
    )
    joined = gathered_copies(
        lax.all_to_all(
            placed.reshape(groups, capacity, normed_cols.shape[1]),
            "sp",
            split_axis=0,
            concat_axis=0,
            tiled=True,
        ),
        "tp",
        2,
    )
    slot_count = joined.shape[0] * joined.shape[1]
    flat_rows = joined.reshape(slot_count, joined.shape[2])
    gate_act = jnp.einsum(
        "rd,edf->ref", flat_rows, gate_weight[0], preferred_element_type=jnp.float32
    )
    up_act = jnp.einsum("rd,edf->ref", flat_rows, up_weight[0], preferred_element_type=jnp.float32)
    scaled = (
        lax.all_to_all(routed_weights, "sp", split_axis=0, concat_axis=0, tiled=True)
        .reshape(slot_count, EPG)
        .astype(jnp.float32)[:, :, None]
    )
    hidden = (jax.nn.silu(gate_act) * up_act * scaled).astype(jnp.bfloat16)
    partials = jnp.einsum("ref,efd->rd", hidden, down_weight[0], preferred_element_type=jnp.float32)
    partials = partials.reshape(joined.shape)
    summed_rows = sum_at_owner(partials.astype(jnp.bfloat16), "tp", 2).astype(jnp.bfloat16)
    returned_rows = lax.all_to_all(summed_rows, "sp", split_axis=0, concat_axis=0, tiled=True)
    moe_rows = returned_rows.reshape(groups * capacity, quarter)[slot_index]
    return (stream_cols.astype(jnp.float32) + moe_rows.astype(jnp.float32)).astype(jnp.bfloat16)


def solution(mesh):
    placed = (
        P("sp", "tp"),
        P("sp", "tp"),
        P("sp", None),
        P("sp", None),
        P(),
        P(None, "tp"),
        P(None, "tp"),
        P(None, "tp"),
        P(None, "tp"),
        P("tp", None),
        P("tp", None),
        P("sp", None),
        P(),
        P("sp"),
        P("sp", None),
        P("sp"),
        P("sp", None),
        P("sp", None, None, "tp"),
        P("sp", None, None, "tp"),
        P("sp", None, "tp", None),
    )
    return jax.shard_map(body, mesh=mesh, in_specs=placed, out_specs=P("sp", "tp"), check_vma=False)
```

time: 335 us -> 188 us (0.56)
  waiting for transfers between devices: 144 us -> 46.7 us
  local copies, waits for them, and re-layouts: 57.4 us -> 13.8 us
  Pallas kernels: 0 us -> 35.1 us
  between operations: 13.9 us -> 0.29 us
  starting transfers between devices: 59.7 us -> 47 us
  matrix products: 12.9 us -> 5.55 us
  loops' own time: 5.7 us -> 0 us
    all_gather x1 -> x0, waiting for transfers between devices: 97.5 us -> none  [sent_together(): result = lax.all_gather(both, axis, axis=dim, tiled=True)]
    pallas_call x0 -> x1, Pallas kernels: none -> 35.1 us  [attention(): pl.pallas_call(attention_kernel, out_shape=jax.ShapeDtypeStruct((384, BLO...]
    while x23 -> x0, local copies, waits for them, and re-layouts: 23.1 us -> none  [the longest x7 23 us: body(): lax.fori_loop(0, total_rows // block_rows, visit_block, start_state)]
    split x3 -> x0, local copies, waits for them, and re-layouts: 13.6 us -> none  [sent_together(): jnp.split(result, [sum(widths[:k]) for k in range(1, len(widths))], axis=...]
    all_to_all x1, starting transfers between devices: 42.6 us -> 29.8 us  [body(): lax.all_to_all(routed_weights, 'sp', split_axis=0, concat_axis=0, tiled=T...]
    dot_general x12 -> x1, matrix products: 9.04 us -> 1.58 us  [body(): lax.dot_general(att, jnp.concatenate([out_wide, out_narrow], axis=0), (((...]
    another operation x9 -> x0, loops' own time: 5.7 us -> none  [the longest x1 5.32 us: body(): lax.fori_loop(0, total_rows // block_rows, visit_block, start_state)]
    slice x9 -> x0, local copies, waits for them, and re-layouts: 4.91 us -> none  [the longest x8 4.9 us: visit_block(): query_pos[-1]]
  transfers between devices with their start and end apart: 6 -> 5, of which waited for: 6 -> 5; matrix products, arithmetic and copies ran while one was open for 2% -> 3% of each run, Pallas kernels for 0% -> 0%
where the time goes in v1:
time: 188 us; the launch traced here: 187 us
  starting transfers between devices  47 us (25%)
  waiting for transfers between devices  46.7 us (25%)
  Pallas kernels  35.1 us (19%)
  blocking collectives  33.2 us (18%)
  local copies, waits for them, and re-layouts  13.8 us (7%)
  matrix products  5.55 us (3%)
  other arithmetic  5.49 us (3%)
    pallas_call x1, Pallas kernels, attention(): pl.pallas_call(attention_kernel, out_shape=jax.ShapeDtypeStruct((384, BLO...  35.1 us
    all_to_all x1, starting transfers between devices, body(): lax.all_to_all(routed_weights, 'sp', split_axis=0, concat_axis=0, tiled=T...  29.8 us
    all_to_all x1, blocking collectives, body(): lax.all_to_all(placed.reshape(groups, capacity, normed_cols.shape[1]), 's...  16.8 us
    all_to_all x1, blocking collectives, sum_at_owner(): lax.all_to_all(blocks, axis, split_axis=0, concat_axis=0, tiled=True)  16.5 us
    all_to_all x2, waiting for transfers between devices, sent_to_all(): return lax.all_to_all(copies, axis, split_axis=0, concat_axis=0, tiled=True)  15.5 us
    all_to_all x1, waiting for transfers between devices, body(): lax.all_to_all(summed_rows, 'sp', split_axis=0, concat_axis=0, tiled=True)  13.1 us
    all_to_all x1, waiting for transfers between devices, sum_at_owner(): lax.all_to_all(blocks, axis, split_axis=0, concat_axis=0, tiled=True)  9.37 us
    all_to_all x1, waiting for transfers between devices, body(): lax.all_to_all(routed_weights, 'sp', split_axis=0, concat_axis=0, tiled=T...  8.78 us
  transfers between devices with their start and end apart: 5, of which 5 were waited for; matrix products, arithmetic and copies ran while one was open for 3% of the time, Pallas kernels for 0%

profile of v1, /device:TPU:1, one launch (start us, length us, event | category | flops | bytes accessed | tf_op | source)
XLA Modules:
  0.0 187.2 jit_solution(3235499792196119652)
XLA Ops:
  0.0 0.0 copy-start
  0.0 0.0 copy-start.6
  0.0 0.3 fusion.31
  0.3 0.1 copy.96
  0.4 0.7 copy.97.cos_ref
  1.2 0.8 copy.93
  2.0 0.7 pad_maximum_fusion.1.rope_ref
  2.7 0.7 pad_maximum_fusion.sin_ref
  3.4 35.1 %attention.1 = bf16[384,128]{1,0:T(8,128)(2,1)} custom-call(bf16[128,384]{1,0:T(8,128)(2,1)} %qw_ref.1, bf16[128,256]{1,0:T(8,128)(2,1)} %qn_ref.1, bf16[128,512]{1,0:T(8,128)(2,1)} %latent_ref.1, bf16[128,128]{1,0:T(8,128)(2,1)} %pad_maximum_fusion.1.rope_ref, f32[1,512]{1,0:T(1,128)} %bitcast.53, bf16[512,256]{1,0:T(8,128)(2,1)} %wbk_ref.1, ...), custom_call_target="tpu_custom_call" | custom-call | tf_op jit(solution)/shard_map/attention/pallas_call | solution.py:338
  38.5 0.0 copy-done.6
  38.5 0.0 copy-start.2
  38.6 0.0 copy-start.1
  38.6 0.0 copy-start.4
  38.6 1.6 convolution_convert_fusion
  40.2 0.0 copy-start.3
  40.2 0.8 copy.121
  41.0 4.2 %all-to-all-start = ((bf16[4,128,512]{2,1,0:T(8,128)(2,1)}), bf16[4,128,512]{2,1,0:T(8,128)(2,1)S(1)}, u32[]{:S(2)}, u32[]{:S(2)}) async-start(bf16[4,128,512]{2,1,0:T(8,128)(2,1)} %bitcast.45), calls=%async_computation | async-start | bytes 1048576 | tf_op jit(solution)/shard_map/all_to_all | solution.py:30
  45.2 0.0 copy-done.2
  45.2 0.1 fusion.28
  45.3 0.2 reduce_window_sum.11
  45.5 0.2 select_reduce_fusion
  45.6 0.0 copy-done.1
  45.7 0.0 copy-done.4
  45.7 9.4 %all-to-all-done = bf16[4,128,512]{2,1,0:T(8,128)(2,1)S(1)} async-done(((bf16[4,128,512]{2,1,0:T(8,128)(2,1)}), bf16[4,128,512]{2,1,0:T(8,128)(2,1)S(1)}, u32[]{:S(2)}, u32[]{:S(2)}) %all-to-all-start) | async-done | bytes 524320 | tf_op jit(solution)/shard_map/all_to_all | solution.py:30
  55.1 0.1 convert_reduce_fusion
  55.1 1.0 fusion.18
  56.2 0.6 broadcast_in_dim.15
  56.8 3.2 %all-to-all-start.1 = ((f32[4,1,128]{2,1,0:T(1,128)}), f32[4,1,128]{2,1,0:T(1,128)S(1)}, u32[]{:S(2)}, u32[]{:S(2)}) async-start(f32[4,1,128]{2,1,0:T(1,128)} %broadcast_in_dim.15), calls=%async_computation.1 | async-start | bytes 4096 | tf_op jit(solution)/shard_map/all_to_all | solution.py:36
  60.0 0.0 copy-done.3
  60.1 0.8 dynamic_slice.7
  60.8 0.1 copy.101
  61.0 0.9 scatter_custom_fusion.1
  61.9 1.1 copy.103
  63.0 1.1 all-to-all-done.1
  64.1 29.8 %all-to-all-start.4 = ((bf16[64,4,4]{1,2,0:T(4,128)(2,1)}), bf16[64,4,4]{1,2,0:T(4,128)(2,1)S(1)}, u32[]{:S(2)}, u32[]{:S(2)}) async-start(bf16[64,4,4]{1,2,0:T(4,128)(2,1)} %copy.103), calls=%async_computation.4 | async-start | bytes 131072 | tf_op jit(solution)/shard_map/all_to_all | solution.py:447
  93.9 1.2 scatter_custom_fusion
  95.1 0.1 reshape.87
  95.2 8.8 %all-to-all-done.4 = bf16[64,4,4]{1,2,0:T(4,128)(2,1)S(1)} async-done(((bf16[64,4,4]{1,2,0:T(4,128)(2,1)}), bf16[64,4,4]{1,2,0:T(4,128)(2,1)S(1)}, u32[]{:S(2)}, u32[]{:S(2)}) %all-to-all-start.4) | async-done | bytes 2080 | tf_op jit(solution)/shard_map/all_to_all | solution.py:447
  104.0 16.8 %all_to_all.36 = bf16[64,4,512]{2,1,0:T(4,128)(2,1)S(1)} all-to-all(bf16[64,4,512]{2,1,0:T(4,128)(2,1)S(1)} %reshape.87), channel_id=1, replica_groups=mesh['sp'=64,'tp'=4] {'sp'}, dimensions={0} | all-to-all | bytes 524288 | tf_op jit(solution)/shard_map/all_to_all | solution.py:430
  120.8 1.3 broadcast_in_dim.16
  122.0 3.7 %all-to-all-start.3 = ((bf16[4,64,4,512]{3,2,1,0:T(4,128)(2,1)}), bf16[4,64,4,512]{3,2,1,0:T(4,128)(2,1)S(1)}, u32[]{:S(2)}, u32[]{:S(2)}) async-start(bf16[4,64,4,512]{3,2,1,0:T(4,128)(2,1)} %broadcast_in_dim.16), calls=%async_computation.3 | async-start | bytes 2097152 | tf_op jit(solution)/shard_map/all_to_all | solution.py:36
  125.7 0.1 copy.104
  125.8 0.1 copy.105
  126.0 0.1 reshape.91
  126.1 14.3 %all-to-all-done.3 = bf16[4,64,4,512]{3,2,1,0:T(4,128)(2,1)S(1)} async-done(((bf16[4,64,4,512]{3,2,1,0:T(4,128)(2,1)}), bf16[4,64,4,512]{3,2,1,0:T(4,128)(2,1)S(1)}, u32[]{:S(2)}, u32[]{:S(2)}) %all-to-all-start.3) | async-done | bytes 1048608 | tf_op jit(solution)/shard_map/all_to_all | solution.py:36
  140.4 2.3 %copy.100 = bf16[64,4,4,512]{3,2,1,0:T(4,128)(2,1)} copy(bf16[64,4,4,512]{3,1,0,2:T(4,128)(2,1)S(1)} %bitcast.46) | data formatting | bytes 2097152 | tf_op jit(solution)/shard_map/transpose | solution.py:45
  142.8 1.8 reshape.119
  144.6 0.0 copy-start.5
  144.6 2.5 %fusion.4 = f32[256,4,128]{2,0,1:T(8,128)S(1)} fusion(bf16[256,2048,1]{1,0,2:T(8,128)(2,1)S(1)} %reshape.119, bf16[1,4,2048,128]{3,2,1,0:T(8,128)(2,1)} %param.37), kind=kOutput, calls=%fused_computation.9 | convolution fusion | flops 536870912 | bytes 3670016 | tf_op jit(solution)/shard_map/rd,edf->ref/dot_general | solution.py:442
  147.1 0.0 copy-done.5
  147.1 0.8 fusion.15
  147.9 0.0 copy-done
  147.9 0.7 fusion
  148.6 0.1 copy.120
  148.7 16.5 %all_to_all.37 = bf16[4,64,4,512]{3,1,2,0:T(8,128)(2,1)S(1)} all-to-all(bf16[4,64,4,512]{3,1,2,0:T(8,128)(2,1)S(1)} %bitcast.47), channel_id=1, replica_groups=mesh['sp'=64,'tp'=4] {'tp'}, dimensions={0} | all-to-all | bytes 2097152 | tf_op jit(solution)/shard_map/all_to_all | solution.py:30
  165.2 0.2 reduce_sum.72
  165.4 0.9 copy.109
  166.3 6.1 %all-to-all-start.6 = ((bf16[64,4,512]{2,1,0:T(4,128)(2,1)}), bf16[64,4,512]{2,1,0:T(4,128)(2,1)S(1)}, u32[]{:S(2)}, u32[]{:S(2)}) async-start(bf16[64,4,512]{2,1,0:T(4,128)(2,1)} %copy.109), calls=%async_computation.6 | async-start | bytes 524288 | tf_op jit(solution)/shard_map/all_to_all | solution.py:455
  172.5 13.1 %all-to-all-done.6 = bf16[64,4,512]{2,1,0:T(4,128)(2,1)S(1)} async-done(((bf16[64,4,512]{2,1,0:T(4,128)(2,1)}), bf16[64,4,512]{2,1,0:T(4,128)(2,1)S(1)}, u32[]{:S(2)}, u32[]{:S(2)}) %all-to-all-start.6) | async-done | bytes 262176 | tf_op jit(solution)/shard_map/all_to_all | solution.py:455
  185.6 0.1 reshape.90
  185.6 0.8 gather_fusion
  186.5 0.7 fusion.21
  (10 shorter events, 0.1 us)
Async XLA Ops:
  0.0 147.9 %copy-start = (bf16[1,4,128,2048]{3,2,1,0:T(8,128)(2,1)S(1)}, bf16[1,4,128,2048]{3,2,1,0:T(8,128)(2,1)}, u32[]{:S(2)}) copy-start(bf16[1,4,128,2048]{3,2,1,0:T(8,128)(2,1)} %param.39) | copy-start | bytes 6291460
  0.0 38.5 %copy-start.6 = (bf16[256,2048]{1,0:T(8,128)(2,1)S(1)}, bf16[256,2048]{1,0:T(8,128)(2,1)}, u32[]{:S(2)}) copy-start(bf16[256,2048]{1,0:T(8,128)(2,1)} %param.29) | copy-start | bytes 3145732
  38.5 6.7 %copy-start.2 = (s32[128]{0:T(128)S(1)}, s32[128]{0:T(128)}, u32[]{:S(2)}) copy-start(s32[128]{0:T(128)} %param.33) | copy-start | bytes 1540
  38.6 7.1 %copy-start.1 = (f32[128,2]{0,1:T(2,128)S(1)}, f32[128,2]{0,1:T(2,128)}, u32[]{:S(2)}) copy-start(f32[128,2]{0,1:T(2,128)} %param.36) | copy-start | bytes 3076
  38.6 7.1 %copy-start.4 = (f32[128]{0:T(128)S(1)}, f32[128]{0:T(128)}, u32[]{:S(2)}) copy-start(f32[128]{0:T(128)} %param.35) | copy-start | bytes 1540
  40.2 19.9 %copy-start.3 = (s32[128,2]{0,1:T(2,128)S(1)}, s32[128,2]{0,1:T(2,128)}, u32[]{:S(2)}) copy-start(s32[128,2]{0,1:T(2,128)} %param.34) | copy-start | bytes 3076
  41.0 14.1 %all-to-all-start = ((bf16[4,128,512]{2,1,0:T(8,128)(2,1)}), bf16[4,128,512]{2,1,0:T(8,128)(2,1)S(1)}, u32[]{:S(2)}, u32[]{:S(2)}) async-start(bf16[4,128,512]{2,1,0:T(8,128)(2,1)} %bitcast.45), calls=%async_computation | async-start | bytes 1048576 | tf_op jit(solution)/shard_map/all_to_all | solution.py:30
  56.8 7.4 %all-to-all-start.1 = ((f32[4,1,128]{2,1,0:T(1,128)}), f32[4,1,128]{2,1,0:T(1,128)S(1)}, u32[]{:S(2)}, u32[]{:S(2)}) async-start(f32[4,1,128]{2,1,0:T(1,128)} %broadcast_in_dim.15), calls=%async_computation.1 | async-start | bytes 4096 | tf_op jit(solution)/shard_map/all_to_all | solution.py:36
  64.1 39.9 %all-to-all-start.4 = ((bf16[64,4,4]{1,2,0:T(4,128)(2,1)}), bf16[64,4,4]{1,2,0:T(4,128)(2,1)S(1)}, u32[]{:S(2)}, u32[]{:S(2)}) async-start(bf16[64,4,4]{1,2,0:T(4,128)(2,1)} %copy.103), calls=%async_computation.4 | async-start | bytes 131072 | tf_op jit(solution)/shard_map/all_to_all | solution.py:447
  122.0 18.4 %all-to-all-start.3 = ((bf16[4,64,4,512]{3,2,1,0:T(4,128)(2,1)}), bf16[4,64,4,512]{3,2,1,0:T(4,128)(2,1)S(1)}, u32[]{:S(2)}, u32[]{:S(2)}) async-start(bf16[4,64,4,512]{3,2,1,0:T(4,128)(2,1)} %broadcast_in_dim.16), calls=%async_computation.3 | async-start | bytes 2097152 | tf_op jit(solution)/shard_map/all_to_all | solution.py:36
  144.6 2.5 %copy-start.5 = (bf16[1,4,2048,128]{3,2,1,0:T(8,128)(2,1)S(1)}, bf16[1,4,2048,128]{3,2,1,0:T(8,128)(2,1)}, u32[]{:S(2)}) copy-start(bf16[1,4,2048,128]{3,2,1,0:T(8,128)(2,1)} %param.38) | copy-start | bytes 6291460
  166.3 19.2 %all-to-all-start.6 = ((bf16[64,4,512]{2,1,0:T(4,128)(2,1)}), bf16[64,4,512]{2,1,0:T(4,128)(2,1)S(1)}, u32[]{:S(2)}, u32[]{:S(2)}) async-start(bf16[64,4,512]{2,1,0:T(4,128)(2,1)} %copy.109), calls=%async_computation.6 | async-start | bytes 524288 | tf_op jit(solution)/shard_map/all_to_all | solution.py:455

commit v2 on v1

--- a/solution.py
+++ b/solution.py
@@ -18,47 +18,6 @@
 ROPE_BASE = 10000.0
 EPSILON = 1e-06
 MASKED = -1e30
-
-
-def in_blocks(x, dim, peers):
-    before, after = (x.shape[:dim], x.shape[dim + 1 :])
-    return jnp.moveaxis(x.reshape(*before, peers, -1, *after), dim, 0)
-
-
-def sum_at_owner(x, axis, dim):
-    blocks = in_blocks(x, dim, lax.axis_size(axis))
-    arrived = lax.all_to_all(blocks, axis, split_axis=0, concat_axis=0, tiled=True)
-    return arrived.astype(jnp.float32).sum(axis=0)
-
-
-def sent_to_all(x, axis):
-    copies = jnp.broadcast_to(x, (lax.axis_size(axis), *x.shape))
-    return lax.all_to_all(copies, axis, split_axis=0, concat_axis=0, tiled=True)
-
-
-def of_everyone(x, axis):
-    everything = sent_to_all(x, axis)
-    return jnp.sum(everything, axis=0)
-
-
-def joined_along(blocks, dim):
-    blocks = jnp.moveaxis(blocks, 0, dim)
-    shape = blocks.shape
-    return blocks.reshape(*shape[:dim], shape[dim] * shape[dim + 1], *shape[dim + 2 :])
-
-
-def gathered_copies(x, axis, dim):
-    blocks = sent_to_all(x, axis)
-    return joined_along(blocks, dim)
-
-
-def rms_scale(values, gain_row):
-    widened = values.astype(jnp.float32)
-    return (
-        widened
-        * lax.rsqrt(jnp.mean(widened * widened, axis=-1, keepdims=True) + EPSILON)
-        * gain_row
-    )
 
 
 def angles(positions, width):
@@ -304,7 +263,9 @@
         mixed = functools.reduce(
             jnp.add, [o_recv[j, lo:hi, :].astype(jnp.float32) * (shares[j] / whole) for j in range(XC)]
         )
-        out_ref[lo:hi, :] = mixed.astype(jnp.bfloat16)
+        acc[0, lo:hi, 0:128] = mixed
+    for k in range(3):
+        out_ref[:, k * 128 : (k + 1) * 128] = jnp.transpose(acc[0, k * 128 : (k + 1) * 128, 0:128]).astype(jnp.bfloat16)
 
     q_sibling().wait_send()
     for d in range(1, 4):
@@ -337,7 +298,7 @@
     bf16, f32, dma = jnp.bfloat16, jnp.float32, pltpu.SemaphoreType.DMA
     return pl.pallas_call(
         attention_kernel,
-        out_shape=jax.ShapeDtypeStruct((384, BLOCK), bf16),
+        out_shape=jax.ShapeDtypeStruct((BLOCK, 384), bf16),
         in_specs=[vmem] * 11,
         out_specs=vmem,
         scratch_shapes=[
@@ -361,6 +322,293 @@
         query_wide, query_narrow, latent, jnp.concatenate([rope_key, rope_key], axis=1), gain[None, :],
         wbk, wbv, wsk, wsv, cos, sin,
     )
+
+
+def tail_kernel(
+    att_ref, ow_ref, on_ref, resid_ref, gain_ref, place_ref, cw_ref, gate_hbm, up_hbm, down_hbm,
+    out_ref,
+    gate, up, down, own, stream, far_s, far_r, near_s, comb_s, lb, rb, ss_s, ss_r,
+    cx_s, cx_r, cz_s, cz_r, x_s, x_r, z_s, xg, hidden, part, mfar, mcomb, ml, mr, rz_s, rz_r, rx_s, rx_r,
+    w_sem, p_ss, p_rs, q_ss, q_rs, cx_ss, cx_rs, cz_ss, cz_rs, x_ss, x_rs, z_ss, z_rs,
+    gr_ss, gr_rs, gl_ss, gl_rs, gf_ss, gf_rs, mf_ss, mf_rs, mp_ss, mp_rs, mc_ss, mc_rs,
+    rz_ss, rz_rs, rx_ss, rx_rs,
+):
+    sp = lax.axis_index("sp")
+    tp = lax.axis_index("tp")
+    z = sp // XC
+    xc = lax.rem(sp, XC)
+    right, left, far = lax.rem(tp + 1, 4), lax.rem(tp + 3, 4), lax.rem(tp + 2, 4)
+
+    def x_peer(d):
+        return {"sp": z * XC + lax.rem(xc + d, XC)}
+
+    def z_peer(d):
+        return {"sp": lax.rem(z + d, Z) * XC + xc}
+
+    def send(src, dst, ssem, rsem, to):
+        return pltpu.make_async_remote_copy(
+            src_ref=src, dst_ref=dst, send_sem=ssem, recv_sem=rsem, device_id=to, device_id_type=MESH
+        )
+
+    weights = [
+        pltpu.make_async_copy(gate_hbm, gate, w_sem.at[0]),
+        pltpu.make_async_copy(up_hbm, up, w_sem.at[1]),
+        pltpu.make_async_copy(down_hbm, down, w_sem.at[2]),
+    ]
+    barrier = pltpu.get_barrier_semaphore()
+    for to in (right, left, far):
+        pl.semaphore_signal(barrier, inc=1, device_id={"tp": to}, device_id_type=MESH)
+    for d in range(1, XC):
+        pl.semaphore_signal(barrier, inc=1, device_id=x_peer(d), device_id_type=MESH)
+        pl.semaphore_signal(barrier, inc=1, device_id=z_peer(d), device_id_type=MESH)
+    for copy in weights:
+        copy.start()
+
+    bf16, f32 = jnp.bfloat16, jnp.float32
+    sent = []
+
+    def go(copy):
+        copy.start()
+        sent.append(copy)
+
+    def columns(q):
+        return pl.ds(pl.multiple_of(q * 512, 512), 512)
+
+    def quarter(q):
+        return nn(att_ref[:, 0:256], ow_ref[:, columns(q)]) + nn(att_ref[:, 256:384], on_ref[:, columns(q)])
+
+    far_s[...] = quarter(far).astype(bf16).reshape(far_s.shape)
+    pl.semaphore_wait(barrier, 3 + 2 * (XC - 1))
+
+    go(send(far_s.at[0], far_r.at[0], p_ss.at[0], p_rs.at[0], {"tp": right}))
+    go(send(far_s.at[1], far_r.at[1], p_ss.at[1], p_rs.at[1], {"tp": left}))
+    near_s[0] = quarter(right).astype(bf16).reshape(2, 64, 512)
+    to_right = send(near_s.at[0, 1], lb.at[1], p_ss.at[2], p_rs.at[2], {"tp": right})
+    go(to_right)
+    near_s[1] = quarter(left).astype(bf16).reshape(2, 64, 512)
+    to_left = send(near_s.at[1, 0], rb.at[0], p_ss.at[3], p_rs.at[3], {"tp": left})
+    go(to_left)
+
+    row = lax.broadcasted_iota(jnp.int32, (256, 256), 0)
+    col = lax.broadcasted_iota(jnp.int32, (256, 256), 1)
+    swap = (col == lax.rem(row // 4, 8) * 32 + (row // 32) * 4 + lax.rem(row, 4)).astype(f32).astype(bf16)
+
+    def swapped(block):
+        return nn(swap, block.reshape(256, block.shape[-1])).astype(bf16).reshape(block.shape)
+
+    cx_s[...] = nn(place_ref[...], cw_ref[...]).astype(bf16).reshape(cx_s.shape)
+    for d in range(1, XC):
+        go(send(cx_s.at[d], cx_r.at[d], cx_ss.at[d], cx_rs.at[d], x_peer(d)))
+    cx_r[0] = cx_s[0]
+
+    own[...] = quarter(tp)
+    far_right = send(far_s.at[0], far_r.at[0], p_ss.at[0], p_rs.at[0], {"tp": right})
+    far_right.wait_recv()
+    comb_s[0] = (far_r[0].astype(f32) + near_s[0, 0].astype(f32)).astype(bf16)
+    comb_right = send(comb_s.at[0], lb.at[0], p_ss.at[4], p_rs.at[4], {"tp": right})
+    go(comb_right)
+    far_left = send(far_s.at[1], far_r.at[1], p_ss.at[1], p_rs.at[1], {"tp": left})
+    far_left.wait_recv()
+    comb_s[1] = (far_r[1].astype(f32) + near_s[1, 1].astype(f32)).astype(bf16)
+    comb_left = send(comb_s.at[1], rb.at[1], p_ss.at[5], p_rs.at[5], {"tp": left})
+    go(comb_left)
+
+    for d in range(1, XC):
+        send(cx_s.at[d], cx_r.at[d], cx_ss.at[d], cx_rs.at[d], x_peer(d)).wait_recv()
+    cz_s[...] = swapped(cx_r[...])
+    for d in range(1, Z):
+        go(send(cz_s.at[d], cz_r.at[d], cz_ss.at[d], cz_rs.at[d], z_peer(d)))
+    cz_r[0] = cz_s[0]
+
+    for copy in (to_right, to_left, comb_right, comb_left):
+        copy.wait_recv()
+    share = lb[...].astype(f32).reshape(128, 512) + rb[...].astype(f32).reshape(128, 512) + own[...]
+    rounded = (resid_ref[:, columns(tp)].astype(f32) + share).astype(bf16)
+    stream[...] = rounded.astype(f32)
+    widened = stream[...]
+    squares = jnp.sum(widened * widened, axis=1, keepdims=True)
+    ss_s[...] = jnp.transpose(jnp.broadcast_to(squares, (128, 128)))[0:8, :]
+    squared = [
+        send(ss_s, ss_r.at[k], q_ss.at[k], q_rs.at[k], {"tp": to}) for k, to in enumerate((right, left, far))
+    ]
+    for copy in squared:
+        go(copy)
+    for copy in squared:
+        copy.wait_recv()
+    squares = ss_s[0:1, :] + ss_r[0, 0:1, :] + ss_r[1, 0:1, :] + ss_r[2, 0:1, :]
+    squares = jnp.transpose(jnp.broadcast_to(squares, (128, 128)))[:, 0:1]
+    normed = stream[...] * lax.rsqrt(squares / 2048.0 + EPSILON) * gain_ref[:, columns(tp)]
+    x_s[...] = nn(place_ref[...], normed.astype(bf16)).astype(bf16).reshape(x_s.shape)
+
+    for d in (4, 3, 5, 2, 6, 7, 1):
+        go(send(x_s.at[d], x_r.at[d], x_ss.at[d], x_rs.at[d], x_peer(d)))
+    x_r[0] = x_s[0]
+    for d in range(1, XC):
+        send(x_s.at[d], x_r.at[d], x_ss.at[d], x_rs.at[d], x_peer(d)).wait_recv()
+    z_s[...] = swapped(x_r[...])
+    for d in (1, 7, 2, 6, 3, 5, 4):
+        go(send(z_s.at[d], xg.at[0, d], z_ss.at[d], z_rs.at[d], z_peer(d)))
+    xg[0, 0] = z_s[0]
+
+    order = (0, 1, 7, 2, 6, 3, 5, 4)
+
+    def gather_right(d):
+        return send(xg.at[0, d], xg.at[1, d], gr_ss.at[d], gr_rs.at[d], {"tp": right})
+
+    def gather_left(d):
+        return send(xg.at[0, d], xg.at[3, d], gl_ss.at[d], gl_rs.at[d], {"tp": left})
+
+    def gather_far(n):
+        d = order[n]
+        if n % 2 == 0:
+            return send(xg.at[1, d], xg.at[2, d], gf_ss.at[d], gf_rs.at[d], {"tp": right})
+        return send(xg.at[3, d], xg.at[2, d], gf_ss.at[d], gf_rs.at[d], {"tp": left})
+
+    def pass_on(n):
+        if n % 2 == 0:
+            gather_right(order[n]).wait_recv()
+        else:
+            gather_left(order[n]).wait_recv()
+        go(gather_far(n))
+
+    for n, d in enumerate(order):
+        if d:
+            send(z_s.at[d], xg.at[0, d], z_ss.at[d], z_rs.at[d], z_peer(d)).wait_recv()
+        go(gather_right(d))
+        go(gather_left(d))
+        if n >= 1:
+            pass_on(n - 1)
+    pass_on(7)
+    for d in range(1, Z):
+        send(cz_s.at[d], cz_r.at[d], cz_ss.at[d], cz_rs.at[d], z_peer(d)).wait_recv()
+    for copy in weights:
+        copy.wait()
+    for n, d in enumerate(order):
+        if n % 2 == 0:
+            gather_left(d).wait_recv()
+        else:
+            gather_right(d).wait_recv()
+        gather_far(n).wait_recv()
+
+    rows_of = (tp, left, far, right)
+    scale = cz_r[...].reshape(256, 128).astype(f32)
+    for e in range(EPG):
+        both = jnp.zeros((256, 256), f32)
+        for k in range(4):
+            rows = pl.ds(pl.multiple_of(rows_of[k] * 512, 512), 512)
+            both = both + nn(
+                xg[k].reshape(256, 512), jnp.concatenate([gate[e, rows, :], up[e, rows, :]], axis=1)
+            )
+        g = both[:, 0:128]
+        active = g / (1.0 + jnp.exp(-g)) * both[:, 128:256] * scale[:, e : e + 1]
+        hidden[:, e * 128 : (e + 1) * 128] = active.astype(bf16)
+
+    def expert_out(q):
+        return nn(hidden[...], down[:, :, columns(q)].reshape(512, 512)).astype(bf16).reshape(8, 32, 512)
+
+    back = (4, 3, 5, 2, 6, 1, 7, 0)
+
+    def m_far(n):
+        to = right if n % 2 == 0 else left
+        d = back[n]
+        return send(part.at[2, d], mfar.at[d], mf_ss.at[d], mf_rs.at[d], {"tp": to})
+
+    def m_plain(n):
+        d = back[n]
+        if n % 2 == 0:
+            return send(part.at[3, d], mr.at[d], mp_ss.at[d], mp_rs.at[d], {"tp": left})
+        return send(part.at[1, d], ml.at[d], mp_ss.at[d], mp_rs.at[d], {"tp": right})
+
+    def m_comb(n):
+        d = back[n]
+        if n % 2 == 0:
+            return send(mcomb.at[d], ml.at[d], mc_ss.at[d], mc_rs.at[d], {"tp": right})
+        return send(mcomb.at[d], mr.at[d], mc_ss.at[d], mc_rs.at[d], {"tp": left})
+
+    def z_back(d):
+        return send(rz_s.at[d], rz_r.at[d], rz_ss.at[d], rz_rs.at[d], z_peer(Z - d))
+
+    def x_back(d):
+        return send(rx_s.at[d], rx_r.at[d], rx_ss.at[d], rx_rs.at[d], x_peer(XC - d))
+
+    part[2] = expert_out(far)
+    for n in range(8):
+        go(m_far(n))
+    part[1] = expert_out(right)
+    part[3] = expert_out(left)
+    for n in range(8):
+        go(m_plain(n))
+    part[0] = expert_out(tp)
+
+    def combine_on(n):
+        d = back[n]
+        m_far(n).wait_recv()
+        mcomb[d] = (mfar[d].astype(f32) + part[1 if n % 2 == 0 else 3, d].astype(f32)).astype(bf16)
+        go(m_comb(n))
+
+    def finish_chunk(n):
+        d = back[n]
+        m_plain(n).wait_recv()
+        m_comb(n).wait_recv()
+        total = (part[0, d].astype(f32) + ml[d].astype(f32) + mr[d].astype(f32)).astype(bf16)
+        if d:
+            rz_s[d] = total
+            go(z_back(d))
+        else:
+            rz_r[0] = total
+
+    for n in range(8):
+        combine_on(n)
+        if n >= 2:
+            finish_chunk(n - 2)
+    finish_chunk(6)
+    finish_chunk(7)
+    for d in range(1, Z):
+        z_back(d).wait_recv()
+    rx_s[...] = swapped(rz_r[...])
+    for d in (4, 3, 5, 2, 6, 7, 1):
+        go(x_back(d))
+    rx_r[0] = rx_s[0]
+    for d in range(1, XC):
+        x_back(d).wait_recv()
+    moe = lax.dot_general(
+        place_ref[...], rx_r[...].reshape(256, 512), (((0,), (0,)), ((), ())), preferred_element_type=f32
+    )
+    out_ref[...] = (stream[...] + moe.astype(bf16).astype(f32)).astype(bf16)
+    for copy in sent:
+        copy.wait_send()
+
+
+def tail(att, out_wide, out_narrow, resid, gain, place, combine, gate, up, down):
+    vmem = pl.BlockSpec(memory_space=pltpu.VMEM)
+    hbm = pl.BlockSpec(memory_space=pl.ANY)
+    bf16, f32, dma = jnp.bfloat16, jnp.float32, pltpu.SemaphoreType.DMA
+
+    def chunks(width, *lead):
+        return pltpu.VMEM((*lead, 8, 32, width), bf16)
+
+    half = pltpu.VMEM((2, 64, 512), bf16)
+    return pl.pallas_call(
+        tail_kernel,
+        out_shape=jax.ShapeDtypeStruct((BLOCK, 512), bf16),
+        in_specs=[vmem] * 7 + [hbm] * 3,
+        out_specs=vmem,
+        scratch_shapes=[
+            pltpu.VMEM((4, 2048, 128), bf16), pltpu.VMEM((4, 2048, 128), bf16), pltpu.VMEM((4, 128, 2048), bf16),
+            pltpu.VMEM((128, 512), f32), pltpu.VMEM((128, 512), f32),
+            half, half, pltpu.VMEM((2, 2, 64, 512), bf16), half, half, half,
+            pltpu.VMEM((8, 128), f32), pltpu.VMEM((3, 8, 128), f32),
+            chunks(128), chunks(128), chunks(128), chunks(128),
+            chunks(512), chunks(512), chunks(512), chunks(512, 4), pltpu.VMEM((256, 512), bf16), chunks(512, 4),
+            chunks(512), chunks(512), chunks(512), chunks(512), chunks(512), chunks(512), chunks(512), chunks(512),
+            dma((3,)), dma((6,)), dma((6,)), dma((3,)), dma((3,)),
+            *[dma((8,))] * 24,
+        ],
+        compiler_params=pltpu.CompilerParams(
+            collective_id=1, has_side_effects=True, vmem_limit_bytes=60 * 1024 * 1024
+        ),
+        name="tail",
+    )(att, out_wide, out_narrow, resid, gain[None, :], place, combine, gate, up, down)
 
 
 def body(
@@ -390,71 +638,20 @@
         query_wide, query_narrow, latent, rope_key, latent_norm_weight,
         broad_key_lift, broad_value_lift, slim_key_lift, slim_value_lift,
     )
-    partial_value = lax.dot_general(
-        att, jnp.concatenate([out_wide, out_narrow], axis=0), (((0,), (0,)), ((), ())),
-        preferred_element_type=jnp.float32,
+    token = jnp.arange(local_tokens, dtype=jnp.int32)
+    same = group_route[:, None] == group_route[None, :]
+    rank = jnp.sum((same & (token[None, :] < token[:, None])).astype(jnp.int32), axis=1)
+    own_index = lax.axis_index("sp")
+    dz = (group_route // XC - own_index // XC) % Z
+    dx = (group_route % XC - own_index % XC) % XC
+    slot_index = dx * 32 + dz * 4 + rank
+    place = (jnp.arange(256, dtype=jnp.int32)[:, None] == slot_index[None, :]).astype(jnp.bfloat16)
+    share_of = group_prob[:, None] * expert_prob / jnp.sum(expert_prob, axis=1, keepdims=True)
+    chosen = (expert_pair[:, :, None] == jnp.arange(128, dtype=jnp.int32)[None, None, :]).astype(jnp.float32)
+    combine = jnp.sum(share_of[:, :, None] * chosen, axis=1).astype(jnp.bfloat16)
+    return tail(
+        att, out_wide, out_narrow, resid, ffn_gain, place, combine, gate_weight[0], up_weight[0], down_weight[0]
     )
-    model_width = resid.shape[1]
-    tp_size = lax.axis_size("tp")
-    quarter = model_width // tp_size
-    col_start = lax.axis_index("tp") * quarter
-    share = sum_at_owner(partial_value.astype(jnp.bfloat16), "tp", 1)
-    resid_cols = lax.dynamic_slice_in_dim(resid, col_start, quarter, 1)
-    stream_cols = (resid_cols.astype(jnp.float32) + share).astype(jnp.bfloat16)
-    widened = stream_cols.astype(jnp.float32)
-    square_total = of_everyone(jnp.sum(widened * widened, axis=1), "tp")
-    gain_cols = lax.dynamic_slice_in_dim(ffn_gain, col_start, quarter, 0)
-    normed_cols = (
-        widened * lax.rsqrt(square_total[:, None] / model_width + EPSILON) * gain_cols[None, :]
-    ).astype(jnp.bfloat16)
-    groups = lax.axis_size("sp")
-    capacity = 2 * local_tokens // groups
-    share_of = group_prob[:, None] * expert_prob / jnp.sum(expert_prob, axis=1, keepdims=True)
-    chosen = (expert_pair[:, :, None] == jnp.arange(EPG, dtype=jnp.int32)[None, None, :]).astype(
-        jnp.float32
-    )
-    combine = jnp.sum(share_of[:, :, None] * chosen, axis=1).astype(jnp.bfloat16)
-    member = (group_route[:, None] == jnp.arange(groups, dtype=jnp.int32)[None, :]).astype(
-        jnp.int32
-    )
-    group_rank = jnp.sum(jnp.cumsum(member, axis=0) * member, axis=1) - 1
-    slot_index = group_route * capacity + group_rank
-    routed_weights = jnp.zeros((groups * capacity, EPG), jnp.bfloat16).at[slot_index].set(combine)
-    routed_weights = routed_weights.reshape(groups, capacity, EPG)
-    placed = (
-        jnp.zeros((groups * capacity, normed_cols.shape[1]), jnp.bfloat16)
-        .at[slot_index]
-        .set(normed_cols)
-    )
-    joined = gathered_copies(
-        lax.all_to_all(
-            placed.reshape(groups, capacity, normed_cols.shape[1]),
-            "sp",
-            split_axis=0,
-            concat_axis=0,
-            tiled=True,
-        ),
-        "tp",
-        2,
-    )
-    slot_count = joined.shape[0] * joined.shape[1]
-    flat_rows = joined.reshape(slot_count, joined.shape[2])
-    gate_act = jnp.einsum(
-        "rd,edf->ref", flat_rows, gate_weight[0], preferred_element_type=jnp.float32
-    )
-    up_act = jnp.einsum("rd,edf->ref", flat_rows, up_weight[0], preferred_element_type=jnp.float32)
-    scaled = (
-        lax.all_to_all(routed_weights, "sp", split_axis=0, concat_axis=0, tiled=True)
-        .reshape(slot_count, EPG)
-        .astype(jnp.float32)[:, :, None]
-    )
-    hidden = (jax.nn.silu(gate_act) * up_act * scaled).astype(jnp.bfloat16)
-    partials = jnp.einsum("ref,efd->rd", hidden, down_weight[0], preferred_element_type=jnp.float32)
-    partials = partials.reshape(joined.shape)
-    summed_rows = sum_at_owner(partials.astype(jnp.bfloat16), "tp", 2).astype(jnp.bfloat16)
-    returned_rows = lax.all_to_all(summed_rows, "sp", split_axis=0, concat_axis=0, tiled=True)
-    moe_rows = returned_rows.reshape(groups * capacity, quarter)[slot_index]
-    return (stream_cols.astype(jnp.float32) + moe_rows.astype(jnp.float32)).astype(jnp.bfloat16)
 
 
 def solution(mesh):

time: 188 us -> 135 us (0.72)
  Pallas kernels: 35.1 us -> 128 us
  starting transfers between devices: 47 us -> 0 us
  waiting for transfers between devices: 46.7 us -> 0 us
  blocking collectives: 33.2 us -> 0 us
  local copies, waits for them, and re-layouts: 13.8 us -> 3.26 us
  matrix products: 5.55 us -> 0 us
  other arithmetic: 5.49 us -> 3.38 us
    pallas_call x1 -> x2, Pallas kernels: 35.1 us -> 128 us  [the longest x1 93.1 us: tail(): pl.pallas_call(tail_kernel, out_shape=jax.ShapeDtypeStruct((BLOCK, 512),...]
    all_to_all x5 -> x0, starting transfers between devices: 47 us -> none  [the longest x1 29.8 us: body(): lax.all_to_all(routed_weights, 'sp', split_axis=0, concat_axis=0, tiled=T...]
    all_to_all x5 -> x0, waiting for transfers between devices: 46.7 us -> none  [the longest x2 15.5 us: sent_to_all(): return lax.all_to_all(copies, axis, split_axis=0, concat_axis=0, tiled=True)]
    all_to_all x2 -> x0, blocking collectives: 33.2 us -> none  [the longest x1 16.8 us: body(): lax.all_to_all(placed.reshape(groups, capacity, normed_cols.shape[1]), 's...]
    dot_general x4 -> x0, matrix products: 5.55 us -> none  [the longest x1 2.48 us: body(): jnp.einsum('rd,edf->ref', flat_rows, gate_weight[0], preferred_element_ty...]
    transpose x1 -> x0, local copies, waits for them, and re-layouts: 2.34 us -> none  [joined_along(): blocks = jnp.moveaxis(blocks, 0, dim)]
    reshape x5 -> x0, local copies, waits for them, and re-layouts: 2.2 us -> none  [the longest x1 1.12 us: body(): routed_weights = routed_weights.reshape(groups, capacity, EPG)]
  transfers between devices with their start and end apart: 5 -> 0, of which waited for: 5 -> 0; matrix products, arithmetic and copies ran while one was open for 3% -> 0% of each run, Pallas kernels for 0% -> 0%
where the time goes in v2:
time: 135 us
  Pallas kernels  128 us (95%)
  other arithmetic  3.38 us (3%)
  local copies, waits for them, and re-layouts  3.26 us (2%)
    pallas_call x1, Pallas kernels, tail(): pl.pallas_call(tail_kernel, out_shape=jax.ShapeDtypeStruct((BLOCK, 512),...  93.1 us
    pallas_call x1, Pallas kernels, attention(): pl.pallas_call(attention_kernel, out_shape=jax.ShapeDtypeStruct((BLOCK, 3...  35.2 us

profile of v2, /device:TPU:1, one launch (start us, length us, event | category | flops | bytes accessed | tf_op | source)
XLA Modules:
  0.0 135.0 jit_solution(17983303127086300087)
XLA Ops:
  0.0 0.0 copy-start.2
  0.0 0.0 copy-start
  0.0 0.0 copy-start.3
  0.0 0.0 copy-start.1
  0.0 0.9 copy.35
  0.9 0.7 pad_maximum_fusion.1.rope_ref
  1.6 0.3 fusion.2
  1.9 0.1 copy.38
  2.0 0.7 copy.39.cos_ref
  2.7 0.7 pad_maximum_fusion.sin_ref
  3.5 35.2 %attention.1.att_ref = bf16[128,384]{1,0:T(8,128)(2,1)} custom-call(bf16[128,384]{1,0:T(8,128)(2,1)} %qw_ref.1, bf16[128,256]{1,0:T(8,128)(2,1)} %qn_ref.1, bf16[128,512]{1,0:T(8,128)(2,1)} %latent_ref.1, bf16[128,128]{1,0:T(8,128)(2,1)} %pad_maximum_fusion.1.rope_ref, f32[1,512]{1,0:T(1,128)} %bitcast.11, bf16[512,256]{1,0:T(8,128)(2,1)} %wbk_ref.1, ...), custom_call_target="tpu_custom_call" | custom-call | tf_op jit(solution)/shard_map/attention/pallas_call | solution.py:299
  38.6 0.0 copy-done.2
  38.7 0.2 convert_reduce_fusion
  38.9 0.7 fusion.place_ref
  39.5 0.0 copy-done
  39.5 0.0 copy-done.3
  39.6 0.0 copy-done.1
  39.6 0.7 select_reduce_fusion.cw_ref
  40.3 93.1 %tail.1 = bf16[128,512]{1,0:T(8,128)(2,1)} custom-call(bf16[128,384]{1,0:T(8,128)(2,1)} %attention.1.att_ref, bf16[256,2048]{1,0:T(8,128)(2,1)} %ow_ref.1, bf16[128,2048]{1,0:T(8,128)(2,1)} %on_ref.1, bf16[128,2048]{1,0:T(8,128)(2,1)} %resid_ref.1, f32[1,2048]{1,0:T(1,128)} %bitcast.10, bf16[256,128]{1,0:T(8,128)(2,1)} %fusion.place_ref, ...), custom_call_target="tpu_custom_call" | custom-call | tf_op jit(solution)/shard_map/tail/pallas_call | solution.py:591
  133.4 1.6 %copy.41 = bf16[128,512]{1,0:T(8,128)(2,1)} copy(bf16[128,512]{1,0:T(8,128)(2,1)} %tail.1) | data formatting | bytes 262144
  (6 shorter events, 0.1 us)
Async XLA Ops:
  0.0 38.6 %copy-start.2 = (s32[128]{0:T(128)S(1)}, s32[128]{0:T(128)}, u32[]{:S(2)}) copy-start(s32[128]{0:T(128)} %param.33) | copy-start | bytes 1540
  0.0 39.5 %copy-start = (f32[128,2]{0,1:T(2,128)S(1)}, f32[128,2]{0,1:T(2,128)}, u32[]{:S(2)}) copy-start(f32[128,2]{0,1:T(2,128)} %param.36) | copy-start | bytes 3076
  0.0 39.5 %copy-start.3 = (f32[128]{0:T(128)S(1)}, f32[128]{0:T(128)}, u32[]{:S(2)}) copy-start(f32[128]{0:T(128)} %param.35) | copy-start | bytes 1540
  0.0 39.6 %copy-start.1 = (s32[128,2]{0,1:T(2,128)S(1)}, s32[128,2]{0,1:T(2,128)}, u32[]{:S(2)}) copy-start(s32[128,2]{0,1:T(2,128)} %param.34) | copy-start | bytes 3076

commit v3 on v2

v3 whole, which is shorter than its diff:
```python
import functools

import jax
import jax.numpy as jnp
from jax import lax
from jax.experimental import pallas as pl
from jax.experimental.pallas import tpu as pltpu
from jax.sharding import PartitionSpec as P

PLAIN_WIDTH_WIDE = 128
PLAIN_WIDTH_SLIM = 64
ROPE = 64
VALUE_WIDTH_WIDE = 128
VALUE_WIDTH_SLIM = 64
EPG = 4


ROPE_BASE = 10000.0
EPSILON = 1e-06
MASKED = -1e30


MESH = pl.DeviceIdType.MESH
LOG2E = 1.4426950408889634
Z = 8
XC = 8
BLOCK = 128
A_COUNT = 38
ROWS = ((0, 128), (128, 192), (192, 320), (320, 384))
QUERY = ((0, 256), (384, 512), (128, 384), (512, 640))
KEY = ((0, 256), (512, 640), (256, 512), (640, 768))
WIDE_SCALE = (PLAIN_WIDTH_WIDE + ROPE) ** -0.5 * LOG2E
SLIM_SCALE = (PLAIN_WIDTH_SLIM + ROPE) ** -0.5 * LOG2E


def nt(a, b):
    return lax.dot_general(a, b, (((1,), (1,)), ((), ())), preferred_element_type=jnp.float32)


def nn(a, b):
    return lax.dot_general(a, b, (((1,), (0,)), ((), ())), preferred_element_type=jnp.float32)


def remote(src, dst, send_sem, recv_sem, sp):
    return pltpu.make_async_remote_copy(
        src_ref=src,
        dst_ref=dst,
        send_sem=send_sem,
        recv_sem=recv_sem,
        device_id={"sp": sp},
        device_id_type=MESH,
    )


def attention_part(
    go, entered, lifts,
    qw_ref, qn_ref, latent_ref, rope_ref, gain_ref, wbk_ref, wbv_ref, wsk_ref, wsv_ref, cos_ref, sin_ref,
    att_ref,
    q_all, lat_all, keys, values, acc, peak, total,
    b_s, bs_s, b_r, bs_r, g, gs, far_r, fars_r, comb, combs, lb, lbs, rb, rbs, own,
    q_ss, q_rs, qs_ss, qs_rs, up_ss, up_rs, dn_ss, dn_rs, b_ss, b_rs, bt_ss, bt_rs, o_ss, o_rs, t_ss, t_rs,
):
    bf16, f32 = jnp.bfloat16, jnp.float32
    sp = lax.axis_index("sp")
    z = sp // XC
    xc = lax.rem(sp, XC)
    x = xc // 2
    core = lax.rem(xc, 2)
    base = z * XC
    sibling = base + xc + 1 - 2 * core
    above = lax.rem(sp + XC, Z * XC)
    below = lax.rem(sp + (Z - 1) * XC, Z * XC)
    right = base + lax.rem(x + 1, 4) * 2 + core
    left = base + lax.rem(x + 3, 4) * 2 + core

    lane = lax.broadcasted_iota(jnp.int32, (BLOCK, 128), 1)
    low = lane < 64
    first = lax.rem(lane, 64) < 32
    cos = cos_ref[...]
    sin = sin_ref[...]

    def turned(v):
        swapped = jnp.where(first, pltpu.roll(v, 96, 1), pltpu.roll(v, 32, 1))
        return v * cos + swapped * sin

    v = latent_ref[...].astype(f32)
    v = (v * lax.rsqrt(jnp.mean(v * v, axis=1, keepdims=True) + EPSILON) * gain_ref[...]).astype(bf16)
    lat_all[z, :, 0:512] = v[0:64]
    lat_all[z, :, 512:1024] = v[64:128]
    rope = rope_ref[...].astype(f32)
    rope = turned(jnp.transpose(jnp.concatenate([rope, rope], axis=0)))
    lat_all[z, :, 1024:1152] = jnp.where(low[0:64], rope[0:64], rope[64:128]).astype(bf16)
    q_all[xc, :, 0:128] = qw_ref[:, 0:128]
    middle = qw_ref[:, 128:256].astype(f32)
    last = qw_ref[:, 256:384].astype(f32)
    q_all[xc, :, 128:256] = (turned(jnp.where(low, middle, last)) * WIDE_SCALE).astype(bf16)
    q_all[xc, :, 256:384] = pltpu.roll(jnp.where(low, last, middle), 64, 1).astype(bf16)
    for k in range(2):
        v = qn_ref[:, k * 128 : (k + 1) * 128].astype(f32)
        q_all[xc, :, 384 + k * 128 : 512 + k * 128] = jnp.where(low, v, turned(v) * SLIM_SCALE).astype(bf16)

    entered()

    def ring(slot, h, ssem, rsem, to):
        part = lat_all.at[slot, pl.ds(h * 32, 32)]
        return remote(part, part, ssem, rsem, to)

    def up_copy(s, h):
        return ring(lax.rem(z - s + 1 + Z, Z), h, up_ss.at[s, h], up_rs.at[s, h], above)

    def dn_copy(s, h):
        return ring(lax.rem(z + s - 1, Z), h, dn_ss.at[s, h], dn_rs.at[s, h], below)

    def up_sends(s):
        return (z - s + 1 >= 0) & (z < Z - 1)

    def up_comes(s):
        return z - s >= 0

    def dn_sends(s):
        return lax.rem(z + s - 1, Z) <= 2

    def dn_comes(s):
        return lax.rem(z + s, Z) <= 2

    def start_part(s, h):
        if s <= 4:

            @pl.when(up_sends(s))
            def _():
                up_copy(s, h).start()

        if s <= 3:

            @pl.when(dn_sends(s))
            def _():
                dn_copy(s, h).start()

    def hand_on(s):
        for h in range(2):

            @pl.when(up_comes(s))
            def _(h=h):
                up_copy(s, h).wait_recv()

            if s <= 3:

                @pl.when(dn_comes(s))
                def _(h=h):
                    dn_copy(s, h).wait_recv()

            start_part(s + 1, h)

    start_part(1, 0)
    start_part(1, 1)

    def q_part(slot, h, ssem, rsem, to):
        part = q_all.at[slot, pl.ds(h * 64, 64)]
        return remote(part, part, ssem, rsem, to)

    def x_slot(d):
        return lax.rem(x + d, 4) * 2 + core

    def q_right(h):
        return q_part(xc, h, q_ss.at[h], q_rs.at[h], right)

    def q_left(h):
        return q_part(xc, h, q_ss.at[2 + h], q_rs.at[2 + h], left)

    def q_on(h):
        if h == 0:
            return q_part(x_slot(3), 0, q_ss.at[4], q_rs.at[4], right)
        return q_part(x_slot(1), 1, q_ss.at[5], q_rs.at[5], left)

    def q_sibling(d, h):
        return q_part(x_slot(d), h, qs_ss.at[d, h], qs_rs.at[d, h], sibling)

    go(q_right(0))
    go(q_left(1))
    go(q_right(1))
    go(q_left(0))
    go(q_sibling(0, 0))
    go(q_sibling(0, 1))

    peak[...] = jnp.full(peak.shape, MASKED, f32)
    total[...] = jnp.zeros(total.shape, f32)
    acc[...] = jnp.zeros(acc.shape, f32)

    def project(slot):
        rows = jnp.concatenate([lat_all[slot, :, 0:512], lat_all[slot, :, 512:1024]], axis=0)
        packed = lat_all[slot, :, 1024:1152].astype(f32)
        other = pltpu.roll(packed, 64, 1)
        top = low[0:64]
        rot = jnp.concatenate([jnp.where(top, packed, other), jnp.where(top, other, packed)], axis=0)
        wide = (nn(rows, wbk_ref[...]) * WIDE_SCALE).astype(bf16)
        keys[slot, :, 0:128] = wide[:, 0:128]
        keys[slot, :, 128:256] = jnp.where(low, rot, 0.0).astype(bf16)
        keys[slot, :, 256:384] = jnp.where(low, 0.0, rot).astype(bf16)
        keys[slot, :, 384:512] = wide[:, 128:256]
        slim = nn(rows, wsk_ref[...]) * SLIM_SCALE
        keys[slot, :, 512:640] = jnp.where(low, slim, rot).astype(bf16)
        keys[slot, :, 640:768] = jnp.where(low, pltpu.roll(slim, 64, 1), rot).astype(bf16)
        wide = jnp.transpose(nn(rows, wbv_ref[...])).astype(bf16)
        slim = jnp.transpose(nn(rows, wsv_ref[...])).astype(bf16)
        values[slot, 0:128] = wide[0:128]
        values[slot, 128:192] = slim[0:64]
        values[slot, 192:320] = wide[128:256]
        values[slot, 320:384] = slim[64:128]

    def attend(slot, own_block):
        units = [(c, h) for c in range(4) for h in range(4)]

        def score(unit):
            c, h = unit
            ql, qh = QUERY[h]
            kl, kh = KEY[h]
            s = nt(keys[slot, :, kl:kh], q_all[2 * c : 2 * c + 2, :, ql:qh].reshape(256, qh - ql))
            if own_block:
                key_pos = xc * BLOCK + lax.broadcasted_iota(jnp.int32, (BLOCK, 256), 0)
                query_pos = c * 256 + lax.broadcasted_iota(jnp.int32, (BLOCK, 256), 1)
                s = jnp.where(key_pos <= query_pos, s, MASKED)
            return s

        coming = score(units[0])
        for n, (c, h) in enumerate(units):
            s = coming
            if n + 1 < len(units):
                coming = score(units[n + 1])
            lo, hi = ROWS[h]
            before = peak[c, h : h + 1, :]
            top = jnp.maximum(before, jnp.max(s, axis=0, keepdims=True))
            keep = jnp.exp2(before - top)
            weights = jnp.exp2(s - top)
            peak[c, h : h + 1, :] = top
            total[c, h : h + 1, :] = total[c, h : h + 1, :] * keep + jnp.sum(weights, axis=0, keepdims=True)
            acc[c, lo:hi, :] = acc[c, lo:hi, :] * keep + nn(values[slot, lo:hi, :], weights.astype(bf16))

    for copy in lifts:
        copy.wait()
    project(z)
    hand_on(1)
    q_right(0).wait_recv()
    go(q_on(0))
    q_left(1).wait_recv()
    go(q_on(1))
    go(q_sibling(3, 0))
    go(q_sibling(1, 1))
    q_right(1).wait_recv()
    go(q_sibling(3, 1))
    q_left(0).wait_recv()
    go(q_sibling(1, 0))
    hand_on(2)
    for h in range(2):
        q_on(h).wait_recv()
        go(q_sibling(2, h))

    def needed(i):
        s, up = i // 2 + 1, lax.rem(i, 2) == 0
        slot = jnp.where(up, z - s, z + s - Z)
        return slot, (slot >= 0) & (up | (s <= 3))

    def project_some(lo, hi):
        def some(i, carry):
            slot, wanted = needed(i)

            @pl.when(wanted)
            def _():
                project(slot)

            return carry

        lax.fori_loop(lo, hi, some, 0)

    project_some(0, 4)
    for d in (0, 1, 3, 2):
        for h in range(2):
            q_sibling(d, h).wait_recv()
    attend(z, True)
    hand_on(3)

    def visit(i, carry):
        slot, wanted = needed(i)

        @pl.when(i == 2)
        def _():
            hand_on(4)
            project_some(4, 7)

        @pl.when(wanted)
        def _():
            attend(slot, False)

        return carry

    lax.fori_loop(0, 7, visit, 0)

    def block_of(d, which):
        lanes = pl.ds(pl.multiple_of(which * 128, 128), 128)
        chip = lax.rem(x + d, 4)
        stats = jnp.concatenate([peak[chip, 0:4, lanes], total[chip, 0:4, lanes]], axis=0)
        return [acc[chip, lo:hi, lanes] / stats[4 + h : 5 + h, :] for h, (lo, hi) in enumerate(ROWS)], stats

    def merge(parts, heads=(0, 1, 2, 3)):
        results, tops, wholes = [], [], []
        for h in heads:
            top = functools.reduce(jnp.maximum, [stats[h : h + 1, :] for _, stats in parts])
            shares = [jnp.exp2(stats[h : h + 1, :] - top) * stats[4 + h : 5 + h, :] for _, stats in parts]
            whole = functools.reduce(jnp.add, shares)
            results.append(
                functools.reduce(jnp.add, [rows[h] * (share / whole) for (rows, _), share in zip(parts, shares)])
            )
            tops.append(top)
            wholes.append(whole)
        return results, tops, wholes

    def rows_of(ref):
        return [ref[lo:hi, :].astype(f32) for lo, hi in ROWS]

    def half_rows(ref, h):
        mine = {2 * h: ref[0:128, :].astype(f32), 2 * h + 1: ref[128:192, :].astype(f32)}
        return [mine.get(k) for k in range(4)]

    def b_copy(d):
        return remote(b_s.at[d], b_r.at[lax.rem(d + 0, 4)], b_ss.at[d], b_rs.at[d], sibling)

    def bs_copy(d):
        return remote(bs_s.at[d], bs_r.at[d], bt_ss.at[d], bt_rs.at[d], sibling)

    for d in (2, 1, 3, 0):
        rows, stats = block_of(d, 1 - core)
        bs_s[d] = stats
        for h, (lo, hi) in enumerate(ROWS):
            b_s[d, lo:hi, :] = rows[h].astype(bf16)
        go(bs_copy(d))
        go(b_copy(d))

    def pair(src, ssrc, dst, sdst, k, to):
        return (
            remote(ssrc, sdst, t_ss.at[k], t_rs.at[k], to),
            remote(src, dst, o_ss.at[k], o_rs.at[k], to),
        )

    def half(ref, d, h):
        return ref.at[d, pl.ds(h * 192, 192)]

    hops = [
        pair(half(g, 2, 0), gs.at[2], far_r.at[0], fars_r.at[0], 0, right),
        pair(half(g, 2, 1), gs.at[2], far_r.at[1], fars_r.at[1], 1, left),
        pair(half(g, 1, 1), gs.at[1], lb.at[1], lbs.at[1], 2, right),
        pair(half(g, 3, 0), gs.at[3], rb.at[0], rbs.at[0], 3, left),
        pair(comb.at[0], combs.at[0], lb.at[0], lbs.at[0], 4, right),
        pair(comb.at[1], combs.at[1], rb.at[1], rbs.at[1], 5, left),
    ]

    def start_hop(k):
        for copy in hops[k]:
            go(copy)

    def await_hop(k):
        for copy in hops[k]:
            copy.wait_recv()

    for d in (2, 1, 3, 0):
        bs_copy(d).wait_recv()
        b_copy(d).wait_recv()
        results, tops, wholes = merge([block_of(d, core), (rows_of(b_r.at[d]), bs_r[d])])
        gs[d] = jnp.concatenate(tops + wholes, axis=0)
        for h, (lo, hi) in enumerate(ROWS):
            if d == 0:
                own[lo:hi, :] = results[h]
            else:
                g[d, lo:hi, :] = results[h].astype(bf16)
        if d == 2:
            start_hop(0)
            start_hop(1)
        elif d == 1:
            start_hop(2)
        elif d == 3:
            start_hop(3)
    for h, d in ((0, 1), (1, 3)):
        await_hop(h)
        heads = (2 * h, 2 * h + 1)
        mine = half_rows(g.at[d, pl.ds(h * 192, 192)], h)
        results, tops, wholes = merge([(half_rows(far_r.at[h], h), fars_r[h]), (mine, gs[d])], heads)
        comb[h, 0:128, :] = results[0].astype(bf16)
        comb[h, 128:192, :] = results[1].astype(bf16)
        idle = jnp.zeros((2, 128), f32)
        tops, wholes = jnp.concatenate(tops, axis=0), jnp.concatenate(wholes, axis=0)
        order = [tops, idle, wholes, idle] if h == 0 else [idle, tops, idle, wholes]
        combs[h] = jnp.concatenate(order, axis=0)
        start_hop(4 + h)
    for k in range(2, 6):
        await_hop(k)
    final = []
    for h in range(2):
        mine = [own[lo:hi, :] for lo, hi in ROWS]
        results, _, _ = merge(
            [(mine, gs[0]), (half_rows(lb.at[h], h), lbs[h]), (half_rows(rb.at[h], h), rbs[h])], (2 * h, 2 * h + 1)
        )
        final.append(results)
    att_ref[:, 0:128] = jnp.transpose(final[0][0]).astype(bf16)
    att_ref[:, 128:256] = jnp.transpose(final[1][0]).astype(bf16)
    att_ref[:, 256:384] = jnp.transpose(jnp.concatenate([final[0][1], final[1][1]], axis=0)).astype(bf16)

    for s in range(1, 5):
        for h in range(2):

            @pl.when(up_sends(s))
            def _(s=s, h=h):
                up_copy(s, h).wait_send()

            if s <= 3:

                @pl.when(dn_sends(s))
                def _(s=s, h=h):
                    dn_copy(s, h).wait_send()


def tail_part(
    go, projections, weights,
    att_ref, ow_ref, on_ref, resid, gain_ref, place, cw, gate, up, down, stream_ref, moe_ref,
    own, far_s, far_r, near_s, comb_s, lb, rb, ss_s, ss_r,
    cx_s, cx_r, cz_s, cz_r, x_s, x_r, z_s, xg, hidden, part, mfar, mcomb, ml, mr, rz_s, rz_r, rx_s, rx_r,
    p_ss, p_rs, q_ss, q_rs, cx_ss, cx_rs, cz_ss, cz_rs, x_ss, x_rs, z_ss, z_rs,
    gr_ss, gr_rs, gl_ss, gl_rs, gf_ss, gf_rs, mf_ss, mf_rs, mp_ss, mp_rs, mc_ss, mc_rs,
    rz_ss, rz_rs, rx_ss, rx_rs,
):
    sp = lax.axis_index("sp")
    tp = lax.axis_index("tp")
    z = sp // XC
    xc = lax.rem(sp, XC)
    right, left, far = lax.rem(tp + 1, 4), lax.rem(tp + 3, 4), lax.rem(tp + 2, 4)

    def x_peer(d):
        return {"sp": z * XC + lax.rem(xc + d, XC)}

    def z_peer(d):
        return {"sp": lax.rem(z + d, Z) * XC + xc}

    def send(src, dst, ssem, rsem, to):
        return pltpu.make_async_remote_copy(
            src_ref=src, dst_ref=dst, send_sem=ssem, recv_sem=rsem, device_id=to, device_id_type=MESH
        )

    bf16, f32 = jnp.bfloat16, jnp.float32
    def columns(q):
        return pl.ds(pl.multiple_of(q * 512, 512), 512)

    def quarter(q):
        return nn(att_ref[:, 0:256], ow_ref[:, columns(q)]) + nn(att_ref[:, 256:384], on_ref[:, columns(q)])

    for copy in projections:
        copy.wait()
    far_s[...] = quarter(far).astype(bf16).reshape(far_s.shape)

    go(send(far_s.at[0], far_r.at[0], p_ss.at[0], p_rs.at[0], {"tp": right}))
    go(send(far_s.at[1], far_r.at[1], p_ss.at[1], p_rs.at[1], {"tp": left}))
    near_s[0] = quarter(right).astype(bf16).reshape(2, 64, 512)
    to_right = send(near_s.at[0, 1], lb.at[1], p_ss.at[2], p_rs.at[2], {"tp": right})
    go(to_right)
    near_s[1] = quarter(left).astype(bf16).reshape(2, 64, 512)
    to_left = send(near_s.at[1, 0], rb.at[0], p_ss.at[3], p_rs.at[3], {"tp": left})
    go(to_left)

    row = lax.broadcasted_iota(jnp.int32, (256, 256), 0)
    col = lax.broadcasted_iota(jnp.int32, (256, 256), 1)
    swap = (col == lax.rem(row // 4, 8) * 32 + (row // 32) * 4 + lax.rem(row, 4)).astype(f32).astype(bf16)

    def swapped(block):
        return nn(swap, block.reshape(256, block.shape[-1])).astype(bf16).reshape(block.shape)

    own[...] = quarter(tp)
    far_right = send(far_s.at[0], far_r.at[0], p_ss.at[0], p_rs.at[0], {"tp": right})
    far_right.wait_recv()
    comb_s[0] = (far_r[0].astype(f32) + near_s[0, 0].astype(f32)).astype(bf16)
    comb_right = send(comb_s.at[0], lb.at[0], p_ss.at[4], p_rs.at[4], {"tp": right})
    go(comb_right)
    far_left = send(far_s.at[1], far_r.at[1], p_ss.at[1], p_rs.at[1], {"tp": left})
    far_left.wait_recv()
    comb_s[1] = (far_r[1].astype(f32) + near_s[1, 1].astype(f32)).astype(bf16)
    comb_left = send(comb_s.at[1], rb.at[1], p_ss.at[5], p_rs.at[5], {"tp": left})
    go(comb_left)

    for copy in (to_right, to_left, comb_right, comb_left):
        copy.wait_recv()
    share = lb[...].astype(f32).reshape(128, 512) + rb[...].astype(f32).reshape(128, 512) + own[...]
    rounded = (resid[...].astype(f32) + share).astype(bf16)
    stream_ref[...] = rounded
    widened = rounded.astype(f32)
    scaled = (widened * gain_ref[:, columns(tp)]).astype(bf16)
    x_s[...] = nn(place[...], scaled).astype(bf16).reshape(x_s.shape)
    for d in (4, 3, 5, 2, 6, 7, 1):
        go(send(x_s.at[d], x_r.at[d], x_ss.at[d], x_rs.at[d], x_peer(d)))
    x_r[0] = x_s[0]
    squares = jnp.sum(widened * widened, axis=1, keepdims=True)
    ss_s[...] = jnp.transpose(jnp.broadcast_to(squares, (128, 128)))[0:8, :]
    squared = [
        send(ss_s, ss_r.at[k], q_ss.at[k], q_rs.at[k], {"tp": to}) for k, to in enumerate((right, left, far))
    ]
    for copy in squared:
        go(copy)
    for copy in squared:
        copy.wait_recv()
    squares = ss_s[0:1, :] + ss_r[0, 0:1, :] + ss_r[1, 0:1, :] + ss_r[2, 0:1, :]
    scale = lax.rsqrt(squares / 2048.0 + EPSILON)
    coarse = scale.astype(bf16).astype(f32)
    line = lax.broadcasted_iota(jnp.int32, (128, 128), 0)
    sheet = cw[...] + jnp.where(line == 4, coarse, 0.0) + jnp.where(line == 5, scale - coarse, 0.0)
    cx_s[...] = nt(place[...], sheet.astype(bf16)).astype(bf16).reshape(cx_s.shape)
    for d in range(1, XC):
        go(send(cx_s.at[d], cx_r.at[d], cx_ss.at[d], cx_rs.at[d], x_peer(d)))
    cx_r[0] = cx_s[0]
    for d in range(1, XC):
        send(x_s.at[d], x_r.at[d], x_ss.at[d], x_rs.at[d], x_peer(d)).wait_recv()
    z_s[...] = swapped(x_r[...])
    for d in (1, 7, 2, 6, 3, 5, 4):
        go(send(z_s.at[d], xg.at[0, d], z_ss.at[d], z_rs.at[d], z_peer(d)))
    xg[0, 0] = z_s[0]
    for d in range(1, XC):
        send(cx_s.at[d], cx_r.at[d], cx_ss.at[d], cx_rs.at[d], x_peer(d)).wait_recv()
    cz_s[...] = swapped(cx_r[...])
    for d in range(1, Z):
        go(send(cz_s.at[d], cz_r.at[d], cz_ss.at[d], cz_rs.at[d], z_peer(d)))
    cz_r[0] = cz_s[0]

    order = (0, 1, 7, 2, 6, 3, 5, 4)

    def gather_right(d):
        return send(xg.at[0, d], xg.at[1, d], gr_ss.at[d], gr_rs.at[d], {"tp": right})

    def gather_left(d):
        return send(xg.at[0, d], xg.at[3, d], gl_ss.at[d], gl_rs.at[d], {"tp": left})

    def gather_far(n):
        d = order[n]
        if n % 2 == 0:
            return send(xg.at[1, d], xg.at[2, d], gf_ss.at[d], gf_rs.at[d], {"tp": right})
        return send(xg.at[3, d], xg.at[2, d], gf_ss.at[d], gf_rs.at[d], {"tp": left})

    def pass_on(n):
        if n % 2 == 0:
            gather_right(order[n]).wait_recv()
        else:
            gather_left(order[n]).wait_recv()
        go(gather_far(n))

    for n, d in enumerate(order):
        if d:
            send(z_s.at[d], xg.at[0, d], z_ss.at[d], z_rs.at[d], z_peer(d)).wait_recv()
        go(gather_right(d))
        go(gather_left(d))
        if n >= 5:
            pass_on(n - 5)
    for n in range(3, 8):
        pass_on(n)
    for d in range(1, Z):
        send(cz_s.at[d], cz_r.at[d], cz_ss.at[d], cz_rs.at[d], z_peer(d)).wait_recv()
    for copy in weights:
        copy.wait()
    for n, d in enumerate(order):
        if n % 2 == 0:
            gather_left(d).wait_recv()
        else:
            gather_right(d).wait_recv()
        gather_far(n).wait_recv()

    rows_of = (tp, left, far, right)
    scale = cz_r[...].reshape(256, 128).astype(f32)
    norm = scale[:, 4:5] + scale[:, 5:6]
    for e in range(EPG):
        both = jnp.zeros((256, 256), f32)
        for k in range(4):
            rows = pl.ds(pl.multiple_of(rows_of[k] * 512, 512), 512)
            both = both + nn(
                xg[k].reshape(256, 512), jnp.concatenate([gate[e, rows, :], up[e, rows, :]], axis=1)
            )
        both = both * norm
        g = both[:, 0:128]
        active = g / (1.0 + jnp.exp(-g)) * both[:, 128:256] * scale[:, e : e + 1]
        hidden[:, e * 128 : (e + 1) * 128] = active.astype(bf16)

    def expert_out(q):
        return nn(hidden[...], down[:, :, columns(q)].reshape(512, 512)).astype(bf16).reshape(8, 32, 512)

    back = (4, 3, 5, 2, 6, 1, 7, 0)

    def m_far(n):
        to = right if n % 2 == 0 else left
        d = back[n]
        return send(part.at[2, d], mfar.at[d], mf_ss.at[d], mf_rs.at[d], {"tp": to})

    def m_plain(n):
        d = back[n]
        if n % 2 == 0:
            return send(part.at[3, d], mr.at[d], mp_ss.at[d], mp_rs.at[d], {"tp": left})
        return send(part.at[1, d], ml.at[d], mp_ss.at[d], mp_rs.at[d], {"tp": right})

    def m_comb(n):
        d = back[n]
        if n % 2 == 0:
            return send(mcomb.at[d], ml.at[d], mc_ss.at[d], mc_rs.at[d], {"tp": right})
        return send(mcomb.at[d], mr.at[d], mc_ss.at[d], mc_rs.at[d], {"tp": left})

    def z_back(d):
        return send(rz_s.at[d], rz_r.at[d], rz_ss.at[d], rz_rs.at[d], z_peer(Z - d))

    def x_back(d):
        return send(rx_s.at[d], rx_r.at[d], rx_ss.at[d], rx_rs.at[d], x_peer(XC - d))

    part[2] = expert_out(far)
    for n in range(8):
        go(m_far(n))
    part[1] = expert_out(right)
    part[3] = expert_out(left)
    for n in range(8):
        go(m_plain(n))
    part[0] = expert_out(tp)

    def combine_on(n):
        d = back[n]
        m_far(n).wait_recv()
        mcomb[d] = (mfar[d].astype(f32) + part[1 if n % 2 == 0 else 3, d].astype(f32)).astype(bf16)
        go(m_comb(n))

    def finish_chunk(n):
        d = back[n]
        m_plain(n).wait_recv()
        m_comb(n).wait_recv()
        total = (part[0, d].astype(f32) + ml[d].astype(f32) + mr[d].astype(f32)).astype(bf16)
        if d:
            rz_s[d] = total
            go(z_back(d))
        else:
            rz_r[0] = total

    for n in range(8):
        combine_on(n)
        if n >= 5:
            finish_chunk(n - 5)
    for n in range(3, 8):
        finish_chunk(n)
    for d in range(1, Z):
        z_back(d).wait_recv()
    rx_s[...] = swapped(rz_r[...])
    for d in (4, 3, 5, 2, 6, 7, 1):
        go(x_back(d))
    rx_r[0] = rx_s[0]
    for d in range(1, XC):
        x_back(d).wait_recv()
    moe_ref[...] = lax.dot_general(
        place[...], rx_r[...].reshape(256, 512), (((0,), (0,)), ((), ())), preferred_element_type=f32
    ).astype(bf16)


def routing(route_ref, pair_ref, group_ref, prob_ref, place, cw):
    sp = lax.axis_index("sp")
    f32 = jnp.float32
    line = lax.broadcasted_iota(jnp.int32, (128, 128), 0)
    lane = lax.broadcasted_iota(jnp.int32, (128, 128), 1)
    route = route_ref[...]
    across = jnp.broadcast_to(route, (128, 128))
    down = jnp.transpose(across.astype(f32)).astype(jnp.int32)
    earlier = jnp.where(down == across, 1.0, 0.0) * jnp.where(line < lane, 1.0, 0.0)
    rank = jnp.sum(earlier, axis=0, keepdims=True).astype(jnp.int32)
    dz = ((route >> 3) - sp // XC) & 7
    dx = ((route & 7) - lax.rem(sp, XC)) & 7
    slot = dx * 32 + dz * 4 + rank
    rows = lax.broadcasted_iota(jnp.int32, (256, 128), 0)
    place[...] = jnp.where(rows == slot, 1.0, 0.0).astype(jnp.bfloat16)
    both = prob_ref[0:1, :] + prob_ref[1:2, :]
    sheet = jnp.zeros((128, 128), f32)
    for k in range(2):
        share = group_ref[...] * prob_ref[k : k + 1, :] / both
        sheet = sheet + jnp.where(line == pair_ref[k : k + 1, :], share, 0.0)
    cw[...] = sheet.astype(jnp.bfloat16).astype(f32)


def layer_kernel(
    qw_ref, qn_ref, latent_ref, rope_ref, lgain_ref, cos_ref, sin_ref, route_ref, pair_ref, group_ref, prob_ref, gain_ref,
    wbk_hbm, wbv_hbm, wsk_hbm, wsv_hbm, ow_hbm, on_hbm, resid_hbm, gate_hbm, up_hbm, down_hbm,
    stream_ref, moe_ref,
    wbk, wbv, wsk, wsv, ow, on, resid, gate, up, down, place, cw, att, w_sem, *scratch
):
    sp = lax.axis_index("sp")
    tp = lax.axis_index("tp")
    z = sp // XC
    xc = lax.rem(sp, XC)
    mine = resid_hbm.at[:, pl.ds(pl.multiple_of(tp * 512, 512), 512)]
    pairs = (
        (wbk_hbm, wbk), (wbv_hbm, wbv), (wsk_hbm, wsk), (wsv_hbm, wsv), (ow_hbm, ow), (on_hbm, on), (mine, resid),
        (gate_hbm, gate), (up_hbm, up), (down_hbm, down),
    )
    local = [pltpu.make_async_copy(src, dst, w_sem.at[k]) for k, (src, dst) in enumerate(pairs)]
    barrier = pltpu.get_barrier_semaphore()
    for d in range(1, XC):
        pl.semaphore_signal(
            barrier, inc=1, device_id={"sp": z * XC + lax.rem(xc + d, XC)}, device_id_type=MESH
        )
        pl.semaphore_signal(
            barrier, inc=1, device_id={"sp": lax.rem(z + d, Z) * XC + xc}, device_id_type=MESH
        )
    for d in range(1, 4):
        pl.semaphore_signal(barrier, inc=1, device_id={"tp": lax.rem(tp + d, 4)}, device_id_type=MESH)
    for copy in local:
        copy.start()

    def entered():
        pl.semaphore_wait(barrier, 2 * (XC - 1) + 3)

    sent = []

    def go(copy):
        copy.start()
        sent.append(copy)
        return copy

    attention_part(
        go, entered, local[0:4],
        qw_ref, qn_ref, latent_ref, rope_ref, lgain_ref, wbk, wbv, wsk, wsv, cos_ref, sin_ref, att, *scratch[:A_COUNT]
    )
    routing(route_ref, pair_ref, group_ref, prob_ref, place, cw)
    tail_part(
        go, local[4:7], local[7:10], att, ow, on, resid, gain_ref, place, cw, gate, up, down, stream_ref, moe_ref,
        *scratch[A_COUNT:]
    )
    for copy in sent:
        copy.wait_send()


def layer(vectors, matrices):
    vmem = pl.BlockSpec(memory_space=pltpu.VMEM)
    hbm = pl.BlockSpec(memory_space=pl.ANY)
    bf16, f32, dma = jnp.bfloat16, jnp.float32, pltpu.SemaphoreType.DMA

    def results(*lead, rows=384):
        return [pltpu.VMEM((*lead, rows, BLOCK), bf16), pltpu.VMEM((*lead, 8, BLOCK), f32)]

    def chunks(width, *lead):
        return pltpu.VMEM((*lead, 8, 32, width), bf16)

    half = pltpu.VMEM((2, 64, 512), bf16)
    attention_scratch = [
        pltpu.VMEM((XC, BLOCK, 640), bf16),
        pltpu.VMEM((Z, 64, 1152), bf16),
        pltpu.VMEM((Z, BLOCK, 768), bf16),
        pltpu.VMEM((Z, 384, BLOCK), bf16),
        pltpu.VMEM((4, 384, 256), f32),
        pltpu.VMEM((4, 8, 256), f32),
        pltpu.VMEM((4, 8, 256), f32),
        *results(4), *results(4), *results(4),
        *results(2, rows=192), *results(2, rows=192), *results(2, rows=192), *results(2, rows=192),
        pltpu.VMEM((384, BLOCK), f32),
        dma((6,)), dma((6,)), dma((4, 2)), dma((4, 2)), dma((5, 2)), dma((5, 2)), dma((4, 2)), dma((4, 2)),
        dma((4,)), dma((4,)), dma((4,)), dma((4,)), dma((6,)), dma((6,)), dma((6,)), dma((6,)),
    ]
    assert len(attention_scratch) == A_COUNT
    return pl.pallas_call(
        layer_kernel,
        out_shape=[jax.ShapeDtypeStruct((BLOCK, 512), bf16)] * 2,
        in_specs=[vmem] * 12 + [hbm] * 10,
        out_specs=[vmem] * 2,
        scratch_shapes=[
            *[pltpu.VMEM(m.shape, bf16) for m in matrices[0:6]],
            pltpu.VMEM((BLOCK, 512), bf16),
            *[pltpu.VMEM(m.shape, bf16) for m in matrices[7:10]],
            pltpu.VMEM((256, 128), bf16), pltpu.VMEM((128, 128), f32), pltpu.VMEM((BLOCK, 384), bf16), dma((10,)),
            *attention_scratch,
            pltpu.VMEM((128, 512), f32),
            half, half, pltpu.VMEM((2, 2, 64, 512), bf16), half, half, half,
            pltpu.VMEM((8, 128), f32), pltpu.VMEM((3, 8, 128), f32),
            chunks(128), chunks(128), chunks(128), chunks(128),
            chunks(512), chunks(512), chunks(512), chunks(512, 4), pltpu.VMEM((256, 512), bf16), chunks(512, 4),
            chunks(512), chunks(512), chunks(512), chunks(512), chunks(512), chunks(512), chunks(512), chunks(512),
            dma((6,)), dma((6,)), dma((3,)), dma((3,)),
            *[dma((8,))] * 24,
        ],
        compiler_params=pltpu.CompilerParams(
            collective_id=0, has_side_effects=True, vmem_limit_bytes=60 * 1024 * 1024
        ),
        name="layer",
    )(*vectors, *matrices)


def turn_tables(position):
    lane = jnp.arange(128, dtype=jnp.int32)
    frequency = 1.0 / ROPE_BASE ** ((lane % 32).astype(jnp.float32) * 2.0 / ROPE)
    angle = position.astype(jnp.float32)[:, None] * frequency[None, :]
    sign = jnp.where(lane % 64 < 32, -1.0, 1.0)
    return jnp.cos(angle), jnp.sin(angle) * sign[None, :]


def body(
    query_wide,
    query_narrow,
    latent,
    rope_key,
    latent_norm_weight,
    broad_key_lift,
    broad_value_lift,
    slim_key_lift,
    slim_value_lift,
    out_wide,
    out_narrow,
    resid,
    ffn_gain,
    group_route,
    expert_pair,
    group_prob,
    expert_prob,
    gate_weight,
    up_weight,
    down_weight,
):
    cos, sin = turn_tables(lax.axis_index("sp") * BLOCK + jnp.arange(BLOCK, dtype=jnp.int32))
    stream, moe = layer(
        (
            query_wide, query_narrow, latent, rope_key.T, latent_norm_weight[None, :], cos, sin,
            group_route[None, :], expert_pair.T, group_prob[None, :], expert_prob.T, ffn_gain[None, :],
        ),
        (
            broad_key_lift, broad_value_lift, slim_key_lift, slim_value_lift, out_wide, out_narrow, resid,
            gate_weight[0], up_weight[0], down_weight[0],
        ),
    )
    return (stream.astype(jnp.float32) + moe.astype(jnp.float32)).astype(jnp.bfloat16)


def solution(mesh):
    placed = (
        P("sp", "tp"),
        P("sp", "tp"),
        P("sp", None),
        P("sp", None),
        P(),
        P(None, "tp"),
        P(None, "tp"),
        P(None, "tp"),
        P(None, "tp"),
        P("tp", None),
        P("tp", None),
        P("sp", None),
        P(),
        P("sp"),
        P("sp", None),
        P("sp"),
        P("sp", None),
        P("sp", None, None, "tp"),
        P("sp", None, None, "tp"),
        P("sp", None, "tp", None),
    )
    return jax.shard_map(body, mesh=mesh, in_specs=placed, out_specs=P("sp", "tp"), check_vma=False)
```

time: 135 us -> 106 us (0.79)
  Pallas kernels: 128 us -> 104 us
  local copies, waits for them, and re-layouts: 3.26 us -> 0 us
    pallas_call x2 -> x1, Pallas kernels: 128 us -> 104 us  [layer(): pl.pallas_call(layer_kernel, out_shape=[jax.ShapeDtypeStruct((BLOCK, 512)...]
    unnamed x10 -> x0, local copies, waits for them, and re-layouts: 2.45 us -> none
    concatenate x2 -> x0, other arithmetic: 1.44 us -> none  [the longest x1 0.74 us: attention(): sin = jnp.concatenate([-sin, sin, -sin, sin], axis=1)]
where the time goes in v3:
time: 106 us
  Pallas kernels  104 us (98%)
  other arithmetic  2.64 us (2%)
    pallas_call x1, Pallas kernels, layer(): pl.pallas_call(layer_kernel, out_shape=[jax.ShapeDtypeStruct((BLOCK, 512)...  104 us

profile of v3, /device:TPU:1, one launch (start us, length us, event | category | flops | bytes accessed | tf_op | source)
XLA Modules:
  0.0 106.2 jit_solution(8657607452381664255)
XLA Ops:
  0.0 1.0 fusion
  1.0 103.5 %layer.1 = (bf16[128,512]{1,0:T(8,128)(2,1)}, bf16[128,512]{1,0:T(8,128)(2,1)}) custom-call(bf16[128,384]{1,0:T(8,128)(2,1)} %qw_ref.1, bf16[128,256]{1,0:T(8,128)(2,1)} %qn_ref.1, bf16[128,512]{1,0:T(8,128)(2,1)} %latent_ref.1, bf16[64,128]{1,0:T(8,128)(2,1)} %bitcast.13, f32[1,512]{1,0:T(1,128)} %bitcast.15, f32[128,128]{1,0:T(8,128)} %get-tuple-element.10.cos_ref, ...), custom_call_target="tpu_custom_call" | custom-call | tf_op jit(solution)/shard_map/layer/pallas_call | solution.py:757
  104.5 1.7 %add_convert_fusion = bf16[128,512]{1,0:T(8,128)(2,1)} fusion(bf16[128,512]{1,0:T(8,128)(2,1)} %get-tuple-element.8, bf16[128,512]{1,0:T(8,128)(2,1)} %get-tuple-element.7), kind=kLoop, calls=%fused_computation | loop fusion | flops 262144 | bytes 393216 | tf_op jit(solution)/shard_map/convert_element_type | solution.py:825
  (2 shorter events, 0.0 us)

commit v4 on v3

--- a/solution.py
+++ b/solution.py
@@ -25,7 +25,7 @@
 Z = 8
 XC = 8
 BLOCK = 128
-A_COUNT = 38
+A_COUNT = 40
 ROWS = ((0, 128), (128, 192), (192, 320), (320, 384))
 QUERY = ((0, 256), (384, 512), (128, 384), (512, 640))
 KEY = ((0, 256), (512, 640), (256, 512), (640, 768))
@@ -56,7 +56,7 @@
     go, entered, lifts,
     qw_ref, qn_ref, latent_ref, rope_ref, gain_ref, wbk_ref, wbv_ref, wsk_ref, wsv_ref, cos_ref, sin_ref,
     att_ref,
-    q_all, lat_all, keys, values, acc, peak, total,
+    q_all, lat_all, keys, values, scores, kept, acc, peak, total,
     b_s, bs_s, b_r, bs_r, g, gs, far_r, fars_r, comb, combs, lb, lbs, rb, rbs, own,
     q_ss, q_rs, qs_ss, qs_rs, up_ss, up_rs, dn_ss, dn_rs, b_ss, b_rs, bt_ss, bt_rs, o_ss, o_rs, t_ss, t_rs,
 ):
@@ -207,33 +207,42 @@
         values[slot, 192:320] = wide[128:256]
         values[slot, 320:384] = slim[64:128]
 
-    def attend(slot, own_block):
+    def attend(slots, own_block=False):
         units = [(c, h) for c in range(4) for h in range(4)]
 
-        def score(unit):
-            c, h = unit
+        def score(n):
+            c, h = units[n]
             ql, qh = QUERY[h]
             kl, kh = KEY[h]
-            s = nt(keys[slot, :, kl:kh], q_all[2 * c : 2 * c + 2, :, ql:qh].reshape(256, qh - ql))
-            if own_block:
-                key_pos = xc * BLOCK + lax.broadcasted_iota(jnp.int32, (BLOCK, 256), 0)
-                query_pos = c * 256 + lax.broadcasted_iota(jnp.int32, (BLOCK, 256), 1)
-                s = jnp.where(key_pos <= query_pos, s, MASKED)
-            return s
-
-        coming = score(units[0])
-        for n, (c, h) in enumerate(units):
-            s = coming
-            if n + 1 < len(units):
-                coming = score(units[n + 1])
+            q = q_all[2 * c : 2 * c + 2, :, ql:qh].reshape(256, qh - ql)
+            top = peak[c, h : h + 1, :]
+            kept[c, h : h + 1, :] = top
+            for b, slot in enumerate(slots):
+                s = nt(keys[slot, :, kl:kh], q)
+                if own_block:
+                    key_pos = xc * BLOCK + lax.broadcasted_iota(jnp.int32, (BLOCK, 256), 0)
+                    query_pos = c * 256 + lax.broadcasted_iota(jnp.int32, (BLOCK, 256), 1)
+                    s = jnp.where(key_pos <= query_pos, s, MASKED)
+                scores[n, b * BLOCK : (b + 1) * BLOCK, :] = s
+                top = jnp.maximum(top, jnp.max(s, axis=0, keepdims=True))
+            peak[c, h : h + 1, :] = top
+
+        def add(n):
+            c, h = units[n]
             lo, hi = ROWS[h]
-            before = peak[c, h : h + 1, :]
-            top = jnp.maximum(before, jnp.max(s, axis=0, keepdims=True))
-            keep = jnp.exp2(before - top)
-            weights = jnp.exp2(s - top)
-            peak[c, h : h + 1, :] = top
+            top = peak[c, h : h + 1, :]
+            keep = jnp.exp2(kept[c, h : h + 1, :] - top)
+            weights = jnp.exp2(scores[n, 0 : len(slots) * BLOCK, :] - top)
             total[c, h : h + 1, :] = total[c, h : h + 1, :] * keep + jnp.sum(weights, axis=0, keepdims=True)
-            acc[c, lo:hi, :] = acc[c, lo:hi, :] * keep + nn(values[slot, lo:hi, :], weights.astype(bf16))
+            v = jnp.concatenate([values[slot, lo:hi, :] for slot in slots], axis=1)
+            acc[c, lo:hi, :] = acc[c, lo:hi, :] * keep + nn(v, weights.astype(bf16))
+
+        ahead = 16
+        for n in range(16 + ahead):
+            if n < 16:
+                score(n)
+            if n >= ahead:
+                add(n - ahead)
 
     for copy in lifts:
         copy.wait()
@@ -275,24 +284,33 @@
     for d in (0, 1, 3, 2):
         for h in range(2):
             q_sibling(d, h).wait_recv()
-    attend(z, True)
-    hand_on(3)
-
-    def visit(i, carry):
-        slot, wanted = needed(i)
-
-        @pl.when(i == 2)
+    attend([z], True)
+
+    def visit(s, carry):
+        up, dn = z - s, z + s - Z
+        both = (up >= 0) & (dn >= 0) & (s <= 3)
+
+        @pl.when(s == 2)
+        def _():
+            hand_on(3)
+            project_some(4, 6)
+
+        @pl.when(s == 4)
         def _():
             hand_on(4)
-            project_some(4, 7)
-
-        @pl.when(wanted)
+            project_some(6, 7)
+
+        @pl.when(both)
         def _():
-            attend(slot, False)
+            attend([up, dn])
+
+        @pl.when(jnp.logical_not(both) & ((up >= 0) | ((dn >= 0) & (s <= 3))))
+        def _():
+            attend([jnp.where(up >= 0, up, dn)])
 
         return carry
 
-    lax.fori_loop(0, 7, visit, 0)
+    lax.fori_loop(1, 5, visit, 0)
 
     def block_of(d, which):
         lanes = pl.ds(pl.multiple_of(which * 128, 128), 128)
@@ -744,6 +762,8 @@
         pltpu.VMEM((Z, 64, 1152), bf16),
         pltpu.VMEM((Z, BLOCK, 768), bf16),
         pltpu.VMEM((Z, 384, BLOCK), bf16),
+        pltpu.VMEM((16, 2 * BLOCK, 256), f32),
+        pltpu.VMEM((4, 8, 256), f32),
         pltpu.VMEM((4, 384, 256), f32),
         pltpu.VMEM((4, 8, 256), f32),
         pltpu.VMEM((4, 8, 256), f32),

time: 106 us -> 96.4 us (0.909)
  Pallas kernels: 104 us -> 93.7 us
    pallas_call x1, Pallas kernels: 104 us -> 93.7 us  [layer(): pl.pallas_call(layer_kernel, out_shape=[jax.ShapeDtypeStruct((BLOCK, 512)...]
where the time goes in v4:
time: 96.4 us; the launch traced here: 96.3 us
  Pallas kernels  93.7 us (97%)
  other arithmetic  2.64 us (3%)
    pallas_call x1, Pallas kernels, layer(): pl.pallas_call(layer_kernel, out_shape=[jax.ShapeDtypeStruct((BLOCK, 512)...  93.7 us

profile of v4, /device:TPU:1, one launch (start us, length us, event | category | flops | bytes accessed | tf_op | source)
XLA Modules:
  0.0 96.3 jit_solution(6401783214249172791)
XLA Ops:
  0.0 1.0 %fusion = (f32[128,128]{1,0:T(8,128)}, f32[128,128]{1,0:T(8,128)}) fusion(f32[128]{0:T(128)S(1)} %get-tuple-element.11, f32[128]{0:T(128)S(1)} %get-tuple-element.12, f32[128]{0:T(128)S(1)} %add_convert_fusion.1), kind=kLoop, calls=%fused_computation.3 | loop fusion | flops 32768 | bytes 132608 | tf_op jit(solution)/shard_map/mul | solution.py:809
  1.0 93.7 %layer.1 = (bf16[128,512]{1,0:T(8,128)(2,1)}, bf16[128,512]{1,0:T(8,128)(2,1)}) custom-call(bf16[128,384]{1,0:T(8,128)(2,1)} %qw_ref.1, bf16[128,256]{1,0:T(8,128)(2,1)} %qn_ref.1, bf16[128,512]{1,0:T(8,128)(2,1)} %latent_ref.1, bf16[64,128]{1,0:T(8,128)(2,1)} %bitcast.13, f32[1,512]{1,0:T(1,128)} %bitcast.15, f32[128,128]{1,0:T(8,128)} %get-tuple-element.10.cos_ref, ...), custom_call_target="tpu_custom_call" | custom-call | tf_op jit(solution)/shard_map/layer/pallas_call | solution.py:777
  94.7 1.7 %add_convert_fusion = bf16[128,512]{1,0:T(8,128)(2,1)} fusion(bf16[128,512]{1,0:T(8,128)(2,1)} %get-tuple-element.8, bf16[128,512]{1,0:T(8,128)(2,1)} %get-tuple-element.7), kind=kLoop, calls=%fused_computation | loop fusion | flops 262144 | bytes 393216 | tf_op jit(solution)/shard_map/convert_element_type | solution.py:845
  (2 shorter events, 0.0 us)

commit v5 on v4

--- a/solution.py
+++ b/solution.py
@@ -25,6 +25,7 @@
 Z = 8
 XC = 8
 BLOCK = 128
+ORDER = (4, 3, 5, 2, 6, 1, 7, 0)
 A_COUNT = 40
 ROWS = ((0, 128), (128, 192), (192, 320), (320, 384))
 QUERY = ((0, 256), (384, 512), (128, 384), (512, 640))
@@ -487,6 +488,11 @@
     def swapped(block):
         return nn(swap, block.reshape(256, block.shape[-1])).astype(bf16).reshape(block.shape)
 
+    row = lax.broadcasted_iota(jnp.int32, (128, 128), 0)
+    col = lax.broadcasted_iota(jnp.int32, (128, 128), 1)
+    half_in = (col == lax.rem(row // 4, 8) * 16 + (row // 32) * 4 + lax.rem(row, 4)).astype(f32).astype(bf16)
+    half_out = (col == lax.rem(row // 4, 4) * 32 + (row // 16) * 4 + lax.rem(row, 4)).astype(f32).astype(bf16)
+
     own[...] = quarter(tp)
     far_right = send(far_s.at[0], far_r.at[0], p_ss.at[0], p_rs.at[0], {"tp": right})
     far_right.wait_recv()
@@ -507,9 +513,15 @@
     widened = rounded.astype(f32)
     scaled = (widened * gain_ref[:, columns(tp)]).astype(bf16)
     x_s[...] = nn(place[...], scaled).astype(bf16).reshape(x_s.shape)
-    for d in (4, 3, 5, 2, 6, 7, 1):
-        go(send(x_s.at[d], x_r.at[d], x_ss.at[d], x_rs.at[d], x_peer(d)))
-    x_r[0] = x_s[0]
+    def x_copy(h, d):
+        return send(
+            x_s.at[d, pl.ds(h * 16, 16)], x_r.at[h, d], x_ss.at[h, d], x_rs.at[h, d], x_peer(d)
+        )
+
+    for h in range(2):
+        for d in (4, 3, 5, 2, 6, 7, 1):
+            go(x_copy(h, d))
+        x_r[h, 0] = x_s[0, h * 16 : (h + 1) * 16]
     squares = jnp.sum(widened * widened, axis=1, keepdims=True)
     ss_s[...] = jnp.transpose(jnp.broadcast_to(squares, (128, 128)))[0:8, :]
     squared = [
@@ -528,143 +540,156 @@
     for d in range(1, XC):
         go(send(cx_s.at[d], cx_r.at[d], cx_ss.at[d], cx_rs.at[d], x_peer(d)))
     cx_r[0] = cx_s[0]
-    for d in range(1, XC):
-        send(x_s.at[d], x_r.at[d], x_ss.at[d], x_rs.at[d], x_peer(d)).wait_recv()
-    z_s[...] = swapped(x_r[...])
-    for d in (1, 7, 2, 6, 3, 5, 4):
-        go(send(z_s.at[d], xg.at[0, d], z_ss.at[d], z_rs.at[d], z_peer(d)))
-    xg[0, 0] = z_s[0]
+    def z_copy(n):
+        return send(z_s.at[n], xg.at[0, n], z_ss.at[n], z_rs.at[n], z_peer(ORDER[n]))
+
+    for h in range(2):
+        for d in range(1, XC):
+            x_copy(h, d).wait_recv()
+        z_s[4 * h : 4 * h + 4] = nn(half_in, x_r[h].reshape(128, 512)).astype(bf16).reshape(4, 32, 512)
+        for n in range(4 * h, 4 * h + 4):
+            if ORDER[n]:
+                go(z_copy(n))
+            else:
+                xg[0, n] = z_s[n]
     for d in range(1, XC):
         send(cx_s.at[d], cx_r.at[d], cx_ss.at[d], cx_rs.at[d], x_peer(d)).wait_recv()
     cz_s[...] = swapped(cx_r[...])
-    for d in range(1, Z):
-        go(send(cz_s.at[d], cz_r.at[d], cz_ss.at[d], cz_rs.at[d], z_peer(d)))
-    cz_r[0] = cz_s[0]
-
-    order = (0, 1, 7, 2, 6, 3, 5, 4)
-
-    def gather_right(d):
-        return send(xg.at[0, d], xg.at[1, d], gr_ss.at[d], gr_rs.at[d], {"tp": right})
-
-    def gather_left(d):
-        return send(xg.at[0, d], xg.at[3, d], gl_ss.at[d], gl_rs.at[d], {"tp": left})
+    def cz_copy(n):
+        return send(cz_s.at[n], cz_r.at[n], cz_ss.at[n], cz_rs.at[n], z_peer(ORDER[n]))
+
+    for n in range(7):
+        go(cz_copy(n))
+    cz_r[7] = cz_s[7]
+
+    def gather_right(n):
+        return send(xg.at[0, n], xg.at[1, n], gr_ss.at[n], gr_rs.at[n], {"tp": right})
+
+    def gather_left(n):
+        return send(xg.at[0, n], xg.at[3, n], gl_ss.at[n], gl_rs.at[n], {"tp": left})
 
     def gather_far(n):
-        d = order[n]
         if n % 2 == 0:
-            return send(xg.at[1, d], xg.at[2, d], gf_ss.at[d], gf_rs.at[d], {"tp": right})
-        return send(xg.at[3, d], xg.at[2, d], gf_ss.at[d], gf_rs.at[d], {"tp": left})
+            return send(xg.at[1, n], xg.at[2, n], gf_ss.at[n], gf_rs.at[n], {"tp": right})
+        return send(xg.at[3, n], xg.at[2, n], gf_ss.at[n], gf_rs.at[n], {"tp": left})
 
     def pass_on(n):
         if n % 2 == 0:
-            gather_right(order[n]).wait_recv()
+            gather_right(n).wait_recv()
         else:
-            gather_left(order[n]).wait_recv()
+            gather_left(n).wait_recv()
         go(gather_far(n))
 
-    for n, d in enumerate(order):
-        if d:
-            send(z_s.at[d], xg.at[0, d], z_ss.at[d], z_rs.at[d], z_peer(d)).wait_recv()
-        go(gather_right(d))
-        go(gather_left(d))
-        if n >= 5:
-            pass_on(n - 5)
-    for n in range(3, 8):
-        pass_on(n)
-    for d in range(1, Z):
-        send(cz_s.at[d], cz_r.at[d], cz_ss.at[d], cz_rs.at[d], z_peer(d)).wait_recv()
+    arriving = (1, 2, 3, 0, 7, 5, 6, 4)
+    for k, n in enumerate(arriving):
+        if ORDER[n]:
+            z_copy(n).wait_recv()
+        go(gather_right(n))
+        go(gather_left(n))
+        if k >= 5:
+            pass_on(arriving[k - 5])
+    for k in range(8 - 5, 8):
+        pass_on(arriving[k])
+    for n in range(7):
+        cz_copy(n).wait_recv()
     for copy in weights:
         copy.wait()
-    for n, d in enumerate(order):
-        if n % 2 == 0:
-            gather_left(d).wait_recv()
-        else:
-            gather_right(d).wait_recv()
-        gather_far(n).wait_recv()
 
     rows_of = (tp, left, far, right)
     scale = cz_r[...].reshape(256, 128).astype(f32)
-    norm = scale[:, 4:5] + scale[:, 5:6]
-    for e in range(EPG):
-        both = jnp.zeros((256, 256), f32)
-        for k in range(4):
-            rows = pl.ds(pl.multiple_of(rows_of[k] * 512, 512), 512)
-            both = both + nn(
-                xg[k].reshape(256, 512), jnp.concatenate([gate[e, rows, :], up[e, rows, :]], axis=1)
-            )
-        both = both * norm
-        g = both[:, 0:128]
-        active = g / (1.0 + jnp.exp(-g)) * both[:, 128:256] * scale[:, e : e + 1]
-        hidden[:, e * 128 : (e + 1) * 128] = active.astype(bf16)
-
-    def expert_out(q):
-        return nn(hidden[...], down[:, :, columns(q)].reshape(512, 512)).astype(bf16).reshape(8, 32, 512)
-
-    back = (4, 3, 5, 2, 6, 1, 7, 0)
+
+    def experts(h):
+        factors = scale[h * 128 : (h + 1) * 128]
+        norm = factors[:, 4:5] + factors[:, 5:6]
+        for e in range(EPG):
+            both = jnp.zeros((128, 256), f32)
+            for k in range(4):
+                rows = pl.ds(pl.multiple_of(rows_of[k] * 512, 512), 512)
+                both = both + nn(
+                    xg[k, 4 * h : 4 * h + 4].reshape(128, 512),
+                    jnp.concatenate([gate[e, rows, :], up[e, rows, :]], axis=1),
+                )
+            both = both * norm
+            g = both[:, 0:128]
+            active = g / (1.0 + jnp.exp(-g)) * both[:, 128:256] * factors[:, e : e + 1]
+            hidden[h * 128 : (h + 1) * 128, e * 128 : (e + 1) * 128] = active.astype(bf16)
+
+    def expert_out(q, h):
+        rows = hidden[h * 128 : (h + 1) * 128, :]
+        return nn(rows, down[:, :, columns(q)].reshape(512, 512)).astype(bf16).reshape(4, 32, 512)
 
     def m_far(n):
         to = right if n % 2 == 0 else left
-        d = back[n]
-        return send(part.at[2, d], mfar.at[d], mf_ss.at[d], mf_rs.at[d], {"tp": to})
+        return send(part.at[2, n], mfar.at[n], mf_ss.at[n], mf_rs.at[n], {"tp": to})
 
     def m_plain(n):
-        d = back[n]
         if n % 2 == 0:
-            return send(part.at[3, d], mr.at[d], mp_ss.at[d], mp_rs.at[d], {"tp": left})
-        return send(part.at[1, d], ml.at[d], mp_ss.at[d], mp_rs.at[d], {"tp": right})
+            return send(part.at[3, n], mr.at[n], mp_ss.at[n], mp_rs.at[n], {"tp": left})
+        return send(part.at[1, n], ml.at[n], mp_ss.at[n], mp_rs.at[n], {"tp": right})
 
     def m_comb(n):
-        d = back[n]
         if n % 2 == 0:
-            return send(mcomb.at[d], ml.at[d], mc_ss.at[d], mc_rs.at[d], {"tp": right})
-        return send(mcomb.at[d], mr.at[d], mc_ss.at[d], mc_rs.at[d], {"tp": left})
-
-    def z_back(d):
-        return send(rz_s.at[d], rz_r.at[d], rz_ss.at[d], rz_rs.at[d], z_peer(Z - d))
-
-    def x_back(d):
-        return send(rx_s.at[d], rx_r.at[d], rx_ss.at[d], rx_rs.at[d], x_peer(XC - d))
-
-    part[2] = expert_out(far)
-    for n in range(8):
-        go(m_far(n))
-    part[1] = expert_out(right)
-    part[3] = expert_out(left)
-    for n in range(8):
-        go(m_plain(n))
-    part[0] = expert_out(tp)
+            return send(mcomb.at[n], ml.at[n], mc_ss.at[n], mc_rs.at[n], {"tp": right})
+        return send(mcomb.at[n], mr.at[n], mc_ss.at[n], mc_rs.at[n], {"tp": left})
+
+    def z_back(n):
+        return send(rz_s.at[n], rz_r.at[n], rz_ss.at[n], rz_rs.at[n], z_peer(Z - ORDER[n]))
+
+    def x_back(h, d):
+        return send(
+            rx_s.at[h, d], rx_r.at[d, pl.ds(h * 16, 16)], rx_ss.at[h, d], rx_rs.at[h, d], x_peer(XC - d)
+        )
+
+    for h in range(2):
+        half_of = range(4 * h, 4 * h + 4)
+        for n in half_of:
+            if n % 2 == 0:
+                gather_left(n).wait_recv()
+            else:
+                gather_right(n).wait_recv()
+            gather_far(n).wait_recv()
+        experts(h)
+        part[2, 4 * h : 4 * h + 4] = expert_out(far, h)
+        for n in half_of:
+            go(m_far(n))
+        part[1, 4 * h : 4 * h + 4] = expert_out(right, h)
+        part[3, 4 * h : 4 * h + 4] = expert_out(left, h)
+        for n in half_of:
+            go(m_plain(n))
+        part[0, 4 * h : 4 * h + 4] = expert_out(tp, h)
 
     def combine_on(n):
-        d = back[n]
         m_far(n).wait_recv()
-        mcomb[d] = (mfar[d].astype(f32) + part[1 if n % 2 == 0 else 3, d].astype(f32)).astype(bf16)
+        mcomb[n] = (mfar[n].astype(f32) + part[1 if n % 2 == 0 else 3, n].astype(f32)).astype(bf16)
         go(m_comb(n))
 
     def finish_chunk(n):
-        d = back[n]
         m_plain(n).wait_recv()
         m_comb(n).wait_recv()
-        total = (part[0, d].astype(f32) + ml[d].astype(f32) + mr[d].astype(f32)).astype(bf16)
-        if d:
-            rz_s[d] = total
-            go(z_back(d))
+        total = (part[0, n].astype(f32) + ml[n].astype(f32) + mr[n].astype(f32)).astype(bf16)
+        if ORDER[n]:
+            rz_s[n] = total
+            go(z_back(n))
         else:
-            rz_r[0] = total
+            rz_r[n] = total
 
     for n in range(8):
         combine_on(n)
         if n >= 5:
             finish_chunk(n - 5)
-    for n in range(3, 8):
+    for n in range(8 - 5, 8):
         finish_chunk(n)
-    for d in range(1, Z):
-        z_back(d).wait_recv()
-    rx_s[...] = swapped(rz_r[...])
-    for d in (4, 3, 5, 2, 6, 7, 1):
-        go(x_back(d))
-    rx_r[0] = rx_s[0]
-    for d in range(1, XC):
-        x_back(d).wait_recv()
+    for h in range(2):
+        for n in range(4 * h, 4 * h + 4):
+            if ORDER[n]:
+                z_back(n).wait_recv()
+        rx_s[h] = nn(half_out, rz_r[4 * h : 4 * h + 4].reshape(128, 512)).astype(bf16).reshape(8, 16, 512)
+        for d in (4, 3, 5, 2, 6, 7, 1):
+            go(x_back(h, d))
+        rx_r[0, h * 16 : (h + 1) * 16] = rx_s[h, 0]
+    for h in range(2):
+        for d in range(1, XC):
+            x_back(h, d).wait_recv()
     moe_ref[...] = lax.dot_general(
         place[...], rx_r[...].reshape(256, 512), (((0,), (0,)), ((), ())), preferred_element_type=f32
     ).astype(bf16)
@@ -682,7 +707,10 @@
     rank = jnp.sum(earlier, axis=0, keepdims=True).astype(jnp.int32)
     dz = ((route >> 3) - sp // XC) & 7
     dx = ((route & 7) - lax.rem(sp, XC)) & 7
-    slot = dx * 32 + dz * 4 + rank
+    place_of = jnp.zeros_like(dz)
+    for n, d in enumerate(ORDER):
+        place_of = place_of + jnp.where(dz == d, n, 0)
+    slot = dx * 32 + place_of * 4 + rank
     rows = lax.broadcasted_iota(jnp.int32, (256, 128), 0)
     place[...] = jnp.where(rows == slot, 1.0, 0.0).astype(jnp.bfloat16)
     both = prob_ref[0:1, :] + prob_ref[1:2, :]
@@ -757,6 +785,7 @@
         return pltpu.VMEM((*lead, 8, 32, width), bf16)
 
     half = pltpu.VMEM((2, 64, 512), bf16)
+    halves = pltpu.VMEM((2, 8, 16, 512), bf16)
     attention_scratch = [
         pltpu.VMEM((XC, BLOCK, 640), bf16),
         pltpu.VMEM((Z, 64, 1152), bf16),
@@ -789,10 +818,10 @@
             half, half, pltpu.VMEM((2, 2, 64, 512), bf16), half, half, half,
             pltpu.VMEM((8, 128), f32), pltpu.VMEM((3, 8, 128), f32),
             chunks(128), chunks(128), chunks(128), chunks(128),
-            chunks(512), chunks(512), chunks(512), chunks(512, 4), pltpu.VMEM((256, 512), bf16), chunks(512, 4),
-            chunks(512), chunks(512), chunks(512), chunks(512), chunks(512), chunks(512), chunks(512), chunks(512),
+            chunks(512), halves, chunks(512), chunks(512, 4), pltpu.VMEM((256, 512), bf16), chunks(512, 4),
+            chunks(512), chunks(512), chunks(512), chunks(512), chunks(512), chunks(512), halves, chunks(512),
             dma((6,)), dma((6,)), dma((3,)), dma((3,)),
-            *[dma((8,))] * 24,
+            *[dma((8,))] * 4, *[dma((2, 8))] * 2, *[dma((8,))] * 16, *[dma((2, 8))] * 2,
         ],
         compiler_params=pltpu.CompilerParams(
             collective_id=0, has_side_effects=True, vmem_limit_bytes=60 * 1024 * 1024

time: 96.4 us -> 94.2 us (0.977)
  Pallas kernels: 93.7 us -> 91.4 us
    pallas_call x1, Pallas kernels: 93.7 us -> 91.4 us  [layer(): pl.pallas_call(layer_kernel, out_shape=[jax.ShapeDtypeStruct((BLOCK, 512)...]
where the time goes in v5:
time: 94.2 us; the launch traced here: 94.1 us
  Pallas kernels  91.4 us (97%)
  other arithmetic  2.64 us (3%)
    pallas_call x1, Pallas kernels, layer(): pl.pallas_call(layer_kernel, out_shape=[jax.ShapeDtypeStruct((BLOCK, 512)...  91.4 us

profile of v5, /device:TPU:1, one launch (start us, length us, event | category | flops | bytes accessed | tf_op | source)
XLA Modules:
  0.0 94.1 jit_solution(4825165781126879348)
XLA Ops:
  0.0 1.0 %fusion = (f32[128,128]{1,0:T(8,128)}, f32[128,128]{1,0:T(8,128)}) fusion(f32[128]{0:T(128)S(1)} %get-tuple-element.11, f32[128]{0:T(128)S(1)} %get-tuple-element.12, f32[128]{0:T(128)S(1)} %add_convert_fusion.1), kind=kLoop, calls=%fused_computation.3 | loop fusion | flops 32768 | bytes 132608 | tf_op jit(solution)/shard_map/mul | solution.py:838
  1.0 91.4 %layer.1 = (bf16[128,512]{1,0:T(8,128)(2,1)}, bf16[128,512]{1,0:T(8,128)(2,1)}) custom-call(bf16[128,384]{1,0:T(8,128)(2,1)} %qw_ref.1, bf16[128,256]{1,0:T(8,128)(2,1)} %qn_ref.1, bf16[128,512]{1,0:T(8,128)(2,1)} %latent_ref.1, bf16[64,128]{1,0:T(8,128)(2,1)} %bitcast.13, f32[1,512]{1,0:T(1,128)} %bitcast.15, f32[128,128]{1,0:T(8,128)} %get-tuple-element.10.cos_ref, ...), custom_call_target="tpu_custom_call" | custom-call | tf_op jit(solution)/shard_map/layer/pallas_call | solution.py:806
  92.4 1.7 %add_convert_fusion = bf16[128,512]{1,0:T(8,128)(2,1)} fusion(bf16[128,512]{1,0:T(8,128)(2,1)} %get-tuple-element.8, bf16[128,512]{1,0:T(8,128)(2,1)} %get-tuple-element.7), kind=kLoop, calls=%fused_computation | loop fusion | flops 262144 | bytes 393216 | tf_op jit(solution)/shard_map/convert_element_type | solution.py:874
  (2 shorter events, 0.0 us)
